TPU v7x, 32 devices: a whole 2x2x4 slice. The times are simulated.
32 devices in a mesh: sp: 8 (over z, x), tp: 4 (over y, core).
Axes of the slice: x: 2, y: 2, z: 4, core: 2. Of those that a mesh axis runs over, the one named last changes fastest.
Arguments:
- saved_tokens: bfloat16 [1536, 2048], P('sp'), may hold values from -3.75 to 3.75
- cotangent: bfloat16 [1536, 2048], P('sp'), may hold values from -6 to 6
- routes: int32 [1536, 2], P('sp'), may hold values from 0 to 7, all different within a row; in each aligned block of 192 rows (0 to 191, 192 to 383, ...) at most 96 rows name the same one
- route_weights: float32 [1536, 2], P('sp'), may hold values from 0.2 to 1
- gate_in: bfloat16 [1536, 1024], P('sp', 'tp'), may hold values from -6 to 6
- conv_in: bfloat16 [1536, 1024], P('sp', 'tp'), may hold values from -6 to 6
- value_in: bfloat16 [1536, 1024], P('sp', 'tp'), may hold values from -6 to 6
- conv_taps: float32 [3, 1024], replicated, may hold values from -3.5 to 3.5
- out_weight: bfloat16 [2048, 1024], P(None, 'tp'), may hold values from -0.1875 to 0.1875
- gate_proj: bfloat16 [8, 2048, 2048], P('sp', None, 'tp'), may hold values from -0.125 to 0.125
- up_proj: bfloat16 [8, 2048, 2048], P('sp', None, 'tp'), may hold values from -0.125 to 0.125
- down_proj: bfloat16 [8, 2048, 2048], P('sp', 'tp'), may hold values from -0.125 to 0.125
Outputs:
- gate_proj_grad: float32 [8, 2048, 2048], P('sp', None, 'tp')
- up_proj_grad: float32 [8, 2048, 2048], P('sp', None, 'tp')
- down_proj_grad: float32 [8, 2048, 2048], P('sp', 'tp')
- out_weight_grad: float32 [2048, 1024], P('sp', 'tp')
- token_grad: bfloat16 [1536, 2048], P('sp', 'tp')
- gate_in_grad: bfloat16 [1536, 1024], P('sp', 'tp')
- conv_in_grad: bfloat16 [1536, 1024], P('sp', 'tp')
- value_in_grad: bfloat16 [1536, 1024], P('sp', 'tp')
Inputs may be any that keep to these rules, and one draw needn't show every extreme that they name: `routes`: within each aligned block of 192 tokens at most 96 assignments name one expert, a bound that some block reaches of them; the 2 experts of a token differ.
All inputs are finite; a program needn't handle non-finite values.
Results may differ from a plain program's by a relative error of at most 0.0063.
Values may be sent and summed in bfloat16 or wider, within the bound.
A program may use at most 64 MiB of HBM per device.

v0:
```python
import jax
import jax.numpy as jnp
from jax import lax
from jax.sharding import PartitionSpec as P

CLAMP_LIMIT = 7.0
SILU_ALPHA = 1.702


def contract_rows(left, right):
    return lax.dot_general(
        left, right, (((0,), (0,)), ((), ())), preferred_element_type=jnp.float32
    )


def contract_cols(left, right):
    return lax.dot_general(
        left, right, (((1,), (1,)), ((), ())), preferred_element_type=jnp.float32
    )


def halo(cells, axis):
    count = lax.axis_size(axis)
    ends = count - 1
    above = lax.ppermute(cells[-1:], axis, [(i, (i + 1) % count) for i in range(ends)])
    below = lax.ppermute(cells[:1], axis, [((i + 1) % count, i) for i in range(ends)])
    return jnp.concatenate([above, cells, below], axis=0)


def exchange_groups(partial_value, part_width):
    tp_count = lax.axis_size("tp")
    pairs = tp_count // 2
    me = lax.axis_index("tp")
    side, pair = me % 2, me // 2

    def block(which_pair, which_side):
        return lax.dynamic_slice_in_dim(
            partial_value, (2 * which_pair + which_side) * part_width, part_width, 1
        )

    others = [(i, i ^ 1) for i in range(tp_count)]
    sums = []
    for step in range(1, pairs + 1):
        target = (pair + step) % pairs
        given = block(target, 1 - side).astype(jnp.bfloat16)
        got = lax.ppermute(given, "tp", others)
        sums.append(block(target, side) + got.astype(jnp.float32))
    total = sums[-1]
    for step in range(1, pairs):
        moves = [(i, (i + 2 * step) % tp_count) for i in range(tp_count)]
        got = lax.ppermute(sums[step - 1].astype(jnp.bfloat16), "tp", moves)
        total = total + got.astype(jnp.float32)
    return total


def gather_features(part):
    tp_count = lax.axis_size("tp")
    pairs = tp_count // 2
    me = lax.axis_index("tp")
    side, pair = me % 2, me // 2
    width = part.shape[1]
    others = [(i, i ^ 1) for i in range(tp_count)]
    held = [part]
    for step in range(1, pairs):
        moves = [(i, (i + 2 * step) % tp_count) for i in range(tp_count)]
        held.append(lax.ppermute(part, "tp", moves))
    twins = [lax.ppermute(block, "tp", others) for block in held]
    whole = jnp.zeros((part.shape[0], tp_count * width), part.dtype)
    for step in range(pairs):
        first = 2 * ((pair - step) % pairs)
        whole = lax.dynamic_update_slice_in_dim(whole, held[step], (first + side) * width, 1)
        whole = lax.dynamic_update_slice_in_dim(whole, twins[step], (first + 1 - side) * width, 1)
    return whole


def local(
    saved_tokens,
    cotangent,
    routes,
    route_weights,
    gate_in,
    conv_in,
    value_in,
    conv_taps,
    out_weight,
    gate_proj,
    up_proj,
    down_proj,
):
    tok_rows, model_width = saved_tokens.shape
    top_count = routes.shape[1]
    expert_count = lax.axis_size("sp")
    tp_count = lax.axis_size("tp")
    capacity = 2 * tok_rows * top_count // expert_count
    slots = expert_count * capacity
    part_width = model_width // tp_count
    channels = gate_in.shape[1]
    me_tp = lax.axis_index("tp")
    offset = me_tp * part_width

    routes_t = routes.T
    weights_t = route_weights.T
    experts = lax.broadcasted_iota(jnp.int32, (expert_count, tok_rows), 0)
    chosen = [experts == routes_t[k][None, :] for k in range(top_count)]
    hits = sum(c.astype(jnp.bfloat16) for c in chosen)
    earlier = (
        lax.broadcasted_iota(jnp.int32, (tok_rows, tok_rows), 0)
        < lax.broadcasted_iota(jnp.int32, (tok_rows, tok_rows), 1)
    ).astype(jnp.bfloat16)
    before = jnp.dot(hits, earlier, preferred_element_type=jnp.float32)
    slot_ids = lax.broadcasted_iota(jnp.int32, (slots, tok_rows), 0)
    place = jnp.zeros((slots, tok_rows), jnp.float32)
    weighted = jnp.zeros((slots, tok_rows), jnp.float32)
    for k in range(top_count):
        rank = jnp.sum(jnp.where(chosen[k], before, 0.0), axis=0).astype(jnp.int32)
        here = slot_ids == (routes_t[k] * capacity + rank)[None, :]
        place = jnp.where(here, 1.0, place)
        weighted = jnp.where(here, weights_t[k][None, :], weighted)
    place = place.astype(jnp.bfloat16)
    slot_weight = jnp.sum(weighted, axis=1, keepdims=True)

    own_tokens = lax.dynamic_slice_in_dim(saved_tokens, offset, part_width, 1)
    own_cot = lax.dynamic_slice_in_dim(cotangent, offset, part_width, 1)
    send_tokens = jnp.dot(place, own_tokens, preferred_element_type=jnp.float32).astype(jnp.bfloat16)
    cot_rows = jnp.dot(place, own_cot, preferred_element_type=jnp.float32)
    send_grads = (cot_rows * slot_weight).astype(jnp.bfloat16)

    def dispatched(rows):
        rows = rows.reshape(expert_count, capacity, part_width)
        return lax.all_to_all(rows, "sp", split_axis=0, concat_axis=0, tiled=True)

    arrived_tokens = dispatched(send_tokens)
    arrived_tokens, send_grads = lax.optimization_barrier((arrived_tokens, send_grads))
    arrived_grads = dispatched(send_grads)
    rows_in = gather_features(arrived_tokens.reshape(slots, part_width))
    grads_in = gather_features(arrived_grads.reshape(slots, part_width))

    gate_f32 = gate_in.astype(jnp.float32)
    conv_f32 = conv_in.astype(jnp.float32)
    value_f32 = value_in.astype(jnp.float32)
    my_taps = lax.dynamic_slice_in_dim(conv_taps, me_tp * channels, channels, 1)
    prod_rim = halo(conv_f32 * value_f32, "sp")
    conv_out = my_taps[0] * prod_rim[:-2] + my_taps[1] * prod_rim[1:-1] + my_taps[2] * prod_rim[2:]
    mixed = (gate_f32 * conv_out).astype(jnp.bfloat16)
    mixed = jnp.concatenate([mixed, mixed], axis=1)

    w_gate, w_up, w_down = gate_proj[0], up_proj[0], down_proj[0]
    gate_pre = jnp.dot(rows_in, w_gate, preferred_element_type=jnp.float32)
    up_pre = jnp.dot(rows_in, w_up, preferred_element_type=jnp.float32)
    gate_clip = jnp.minimum(gate_pre, CLAMP_LIMIT)
    up_clip = jnp.clip(up_pre, -CLAMP_LIMIT, CLAMP_LIMIT)
    sigmoid_gate = jax.nn.sigmoid(SILU_ALPHA * gate_clip)
    gated_act = gate_clip * sigmoid_gate
    hidden = ((up_clip + 1.0) * gated_act).astype(jnp.bfloat16)
    grads_in, mixed = lax.optimization_barrier((grads_in, mixed))
    mixed_all = lax.all_gather(mixed, "sp", axis=0, tiled=True)
    d_hidden = contract_cols(grads_in, w_down)
    d_up = jnp.where(jnp.abs(up_pre) < CLAMP_LIMIT, d_hidden * gated_act, 0.0).astype(jnp.bfloat16)
    gate_slope = sigmoid_gate + SILU_ALPHA * gate_clip * sigmoid_gate * (1.0 - sigmoid_gate)
    d_gate = jnp.where(gate_pre < CLAMP_LIMIT, d_hidden * (up_clip + 1.0) * gate_slope, 0.0).astype(
        jnp.bfloat16
    )
    partial_value = contract_cols(d_gate, w_gate) + contract_cols(d_up, w_up)
    shares = exchange_groups(partial_value, part_width).astype(jnp.bfloat16)
    down_grad = contract_rows(hidden, grads_in)
    gate_grad = contract_rows(rows_in, d_gate)
    up_grad = contract_rows(rows_in, d_up)

    returned = dispatched(shares).reshape(slots, part_width)
    combined = contract_rows(place, returned)
    token_grad = (own_cot.astype(jnp.float32) + combined).astype(jnp.bfloat16)
    residual = lax.all_gather(token_grad, "tp", axis=1, tiled=True)

    d_conv_out = jnp.dot(residual, out_weight, preferred_element_type=jnp.float32)
    grad_rim = halo(d_conv_out * gate_f32, "sp")
    d_product = my_taps[0] * grad_rim[2:] + my_taps[1] * grad_rim[1:-1] + my_taps[2] * grad_rim[:-2]
    gate_in_grad = (d_conv_out * conv_out).astype(jnp.bfloat16)
    conv_in_grad = (d_product * value_f32).astype(jnp.bfloat16)
    value_in_grad = (d_product * conv_f32).astype(jnp.bfloat16)

    share = tok_rows // tp_count
    quarter = lax.dynamic_slice_in_dim(residual, me_tp * share, share, 0)
    quarter = quarter.reshape(share, expert_count, model_width // expert_count)
    quarter = lax.all_to_all(
        quarter.transpose(1, 0, 2), "sp", split_axis=0, concat_axis=0, tiled=True
    )
    features = lax.all_gather(quarter, "tp", axis=1, tiled=True)
    features = features.reshape(expert_count * tok_rows, -1)
    out_weight_grad = contract_rows(features, mixed_all[:, :channels])
    return (
        gate_grad[None],
        up_grad[None],
        down_grad[None],
        out_weight_grad,
        token_grad,
        gate_in_grad,
        conv_in_grad,
        value_in_grad,
    )


def solution(mesh):
    in_specs = (
        P("sp", None),
        P("sp", None),
        P("sp", None),
        P("sp", None),
        P("sp", "tp"),
        P("sp", "tp"),
        P("sp", "tp"),
        P(),
        P(None, "tp"),
        P("sp", None, "tp"),
        P("sp", None, "tp"),
        P("sp", "tp", None),
    )
    out_specs = (
        P("sp", None, "tp"),
        P("sp", None, "tp"),
        P("sp", "tp", None),
        P("sp", "tp"),
        P("sp", "tp"),
        P("sp", "tp"),
        P("sp", "tp"),
        P("sp", "tp"),
    )
    return jax.shard_map(local, mesh=mesh, in_specs=in_specs, out_specs=out_specs, check_vma=False)
```

profile of v0, /device:TPU:0, one launch (start us, length us, event | category | flops | bytes accessed | tf_op | source)
XLA Modules:
  0.0 215.5 jit_solution(15205514426126750161)
XLA Ops:
  11.3 7.3 %all-to-all-start = ((bf16[8,96,512]{2,1,0:T(8,128)(2,1)}), bf16[8,96,512]{2,1,0:T(8,128)(2,1)}, u32[]{:S(2)}, u32[]{:S(2)}) async-start(bf16[8,96,512]{2,1,0:T(8,128)(2,1)} %bitcast.7), calls=%async_computation | async-start | bytes 1572864 | tf_op jit(solution)/shard_map/all_to_all | solution.py:130
  18.8 2.4 %multiply_convert_fusion.1 = bf16[768,512]{1,0:T(8,128)(2,1)} fusion(f32[768]{0:T(1024)S(1)} %select_reduce_fusion, s32[192]{0:T(256)S(1)} %bitcast.85, s32[192]{0:T(256)S(1)} %bitcast.81, bf16[192,2048]{1,0:T(8,128)(2,1)} %param.13, s32[]{:T(128)S(6)} %select_n.107), kind=kOutput, calls=%fused_computation.23 | convolution fusion | flops 152518656 | bytes 987652 | tf_op jit(solution)/shard_map/dot_general | solution.py:125
  21.2 17.7 %all-to-all-done = bf16[8,96,512]{2,1,0:T(8,128)(2,1)} async-done(((bf16[8,96,512]{2,1,0:T(8,128)(2,1)}), bf16[8,96,512]{2,1,0:T(8,128)(2,1)}, u32[]{:S(2)}, u32[]{:S(2)}) %all-to-all-start) | async-done | bytes 786464 | tf_op jit(solution)/shard_map/all_to_all | solution.py:130
  40.4 3.6 %all-to-all-start.1 = ((bf16[8,96,512]{2,1,0:T(8,128)(2,1)}), bf16[8,96,512]{2,1,0:T(8,128)(2,1)S(1)}, u32[]{:S(2)}, u32[]{:S(2)}) async-start(bf16[8,96,512]{2,1,0:T(8,128)(2,1)} %bitcast.62), calls=%async_computation.1 | async-start | bytes 1572864 | tf_op jit(solution)/shard_map/all_to_all | solution.py:130
  44.1 3.9 %collective-permute-start.6 = (f32[1,256]{1,0:T(1,128)S(1)}, f32[1,256]{1,0:T(1,128)S(1)}, u32[]{:S(2)}, u32[]{:S(2)}) collective-permute-start(f32[1,256]{1,0:T(1,128)S(1)} %get-tuple-element.28), channel_id=1, source_target_pairs={{0,4},{4,8},{8,12},{12,16},{16,20},{20,24},{24,28},{1,5},{5,9},{9,... | collective-permute-start | bytes 3080 | tf_op jit(solution)/shard_map/ppermute | solution.py:25
  50.3 6.8 %collective-permute-done.1 = bf16[768,512]{1,0:T(8,128)(2,1)} collective-permute-done((bf16[768,512]{1,0:T(8,128)(2,1)}, bf16[768,512]{1,0:T(8,128)(2,1)}, u32[]{:S(2)}, u32[]{:S(2)}) %collective-permute-start.1) | collective-permute-done | bytes 786464 | tf_op jit(solution)/shard_map/ppermute | solution.py:66
  71.3 3.7 %fusion.1 = f32[768,512]{1,0:T(8,128)S(1)} fusion(bf16[768,2048]{1,0:T(8,128)(2,1)} %constant_dynamic-update-slice_fusion.4, bf16[1,2048,512]{2,1,0:T(8,128)(2,1)S(1)} %copy-done.3), kind=kOutput, calls=%fused_computation.5 | convolution fusion | flops 1610612736 | bytes 6815744 | tf_op jit(solution)/shard_map/dot_general | solution.py:149
  75.0 11.4 %collective-permute-done.4 = bf16[768,512]{1,0:T(8,128)(2,1)S(1)} collective-permute-done((bf16[768,512]{1,0:T(8,128)(2,1)S(1)}, bf16[768,512]{1,0:T(8,128)(2,1)S(1)}, u32[]{:S(2)}, u32[]{:S(2)}) %collective-permute-start.4) | collective-permute-done | bytes 786464 | tf_op jit(solution)/shard_map/ppermute | solution.py:66
  86.4 3.7 %fusion.7 = f32[768,512]{1,0:T(8,128)S(1)} fusion(bf16[768,2048]{1,0:T(8,128)(2,1)} %constant_dynamic-update-slice_fusion.4, bf16[1,2048,512]{2,1,0:T(8,128)(2,1)S(1)} %copy-done), kind=kOutput, calls=%fused_computation.11 | convolution fusion | flops 1610612736 | bytes 6815744 | tf_op jit(solution)/shard_map/dot_general | solution.py:148
  92.2 2.8 %select_convert_fusion = (bf16[768,512]{1,0:T(8,128)(2,1)S(1)}, bf16[768,512]{1,0:T(8,128)(2,1)S(1)}) fusion(f32[768,512]{1,0:T(8,128)S(1)} %fusion.1, f32[768,512]{1,0:T(8,128)S(1)} %fusion.7, bf16[768,2048]{1,0:T(8,128)(2,1)S(1)} %constant_dynamic-update-slice_fusion, bf16[1,512,2048]{2,1,0:T(8,128)(2,1)S(1)} %copy-done.11), kind=kOutput, calls=%fused_computation.18 | convolution fusion | flops 1619263488 | bytes 9961472 | tf_op jit(solution)/shard_map/dot_general | solution.py:17
  98.9 2.6 %copy-done.1 = f32[768,2048]{1,0:T(8,128)} copy-done((f32[768,2048]{1,0:T(8,128)}, f32[768,2048]{1,0:T(8,128)S(1)}, u32[]{:S(2)}) %copy-start.1) | copy-done | bytes 6291480
  105.7 2.8 %add_convert_fusion.1 = bf16[768,512]{1,0:T(8,128)(2,1)} fusion(bf16[768,512]{1,0:T(8,128)(2,1)} %collective-permute-done.9, f32[768,2048]{1,0:T(8,128)} %copy-done.1, s32[]{:T(128)S(6)} %select_n.125), kind=kLoop, calls=%fused_computation.14 | loop fusion | flops 1179648 | bytes 3145732 | tf_op jit(solution)/shard_map/convert_element_type | solution.py:51
  110.0 18.6 %collective-permute-done.10 = bf16[768,512]{1,0:T(8,128)(2,1)} collective-permute-done((bf16[768,512]{1,0:T(8,128)(2,1)}, bf16[768,512]{1,0:T(8,128)(2,1)}, u32[]{:S(2)}, u32[]{:S(2)}) %collective-permute-start.10) | collective-permute-done | bytes 786464 | tf_op jit(solution)/shard_map/ppermute | solution.py:51
  128.6 3.1 %add_convert_fusion = bf16[768,512]{1,0:T(8,128)(2,1)} fusion(bf16[768,512]{1,0:T(8,128)(2,1)} %collective-permute-done.10, bf16[768,512]{1,0:T(8,128)(2,1)} %collective-permute-done.8, f32[768,2048]{1,0:T(8,128)} %copy-done.1, s32[]{:T(128)S(6)} %select_n.122), kind=kLoop, calls=%fused_computation.13 | loop fusion | flops 1966080 | bytes 3932164 | tf_op jit(solution)/shard_map/convert_element_type | solution.py:164
  131.7 9.7 %all-to-all-start.2 = ((bf16[8,96,512]{2,1,0:T(8,128)(2,1)}), bf16[8,96,512]{2,1,0:T(8,128)(2,1)}, u32[]{:S(2)}, u32[]{:S(2)}) async-start(bf16[8,96,512]{2,1,0:T(8,128)(2,1)} %bitcast.23), calls=%async_computation.2 | async-start | bytes 1572864 | tf_op jit(solution)/shard_map/all_to_all | solution.py:130
  142.2 6.9 %convolution_bitcast_fusion = f32[1,512,2048]{2,1,0:T(8,128)} fusion(bf16[768,2048]{1,0:T(8,128)(2,1)} %copy-done.2, f32[768,512]{1,0:T(8,128)} %copy-done.12, f32[768,512]{1,0:T(8,128)} %copy-done.13), kind=kOutput, calls=%fused_computation.1 | convolution fusion | flops 1614544896 | bytes 10485760 | tf_op jit(solution)/shard_map/dot_general | solution.py:11
  149.0 5.7 %convolution_bitcast_fusion.1 = f32[1,2048,512]{2,1,0:T(8,128)} fusion(bf16[768,2048]{1,0:T(8,128)(2,1)} %constant_dynamic-update-slice_fusion.4, bf16[768,512]{1,0:T(8,128)(2,1)S(1)} %get-tuple-element.20), kind=kOutput, calls=%fused_computation.2 | convolution fusion | flops 1610612736 | bytes 8126464 | tf_op jit(solution)/shard_map/dot_general | solution.py:11
  154.8 11.9 %all-to-all-done.2 = bf16[8,96,512]{2,1,0:T(8,128)(2,1)} async-done(((bf16[8,96,512]{2,1,0:T(8,128)(2,1)}), bf16[8,96,512]{2,1,0:T(8,128)(2,1)}, u32[]{:S(2)}, u32[]{:S(2)}) %all-to-all-start.2) | async-done | bytes 786464 | tf_op jit(solution)/shard_map/all_to_all | solution.py:130
  169.0 8.0 %all_gather.9 = bf16[192,2048]{1,0:T(8,128)(2,1)S(1)} all-gather(bf16[192,512]{1,0:T(8,128)(2,1)S(1)} %fusion.9), channel_id=1, replica_groups=mesh['sp'=8,'tp'=4] {'tp'}, dimensions={1}, use_global_device_ids=true | all-gather | bytes 983040 | tf_op jit(solution)/shard_map/all_gather | solution.py:172
  179.4 4.5 %collective-permute-start.12 = (f32[1,256]{1,0:T(1,128)S(1)}, f32[1,256]{1,0:T(1,128)S(1)}, u32[]{:S(2)}, u32[]{:S(2)}) collective-permute-start(f32[1,256]{1,0:T(1,128)S(1)} %get-tuple-element.25), channel_id=1, source_target_pairs={{0,4},{4,8},{8,12},{12,16},{16,20},{20,24},{24,28},{1,5},{5,9},{9,... | collective-permute-start | bytes 3080 | tf_op jit(solution)/shard_map/ppermute | solution.py:25
  184.7 3.6 %all-to-all-start.3 = ((bf16[8,48,256]{2,1,0:T(8,128)(2,1)}), bf16[8,48,256]{2,1,0:T(8,128)(2,1)S(1)}, u32[]{:S(2)}, u32[]{:S(2)}) async-start(bf16[8,48,256]{2,1,0:T(8,128)(2,1)} %copy.24), calls=%async_computation.3 | async-start | bytes 393216 | tf_op jit(solution)/shard_map/all_to_all | solution.py:184
  188.4 5.9 %convolution_bitcast_fusion.2 = f32[1,2048,512]{2,1,0:T(8,128)} fusion(bf16[768,2048]{1,0:T(8,128)(2,1)} %constant_dynamic-update-slice_fusion.4, bf16[768,512]{1,0:T(8,128)(2,1)} %copy-done.5), kind=kOutput, calls=%fused_computation.3 | convolution fusion | flops 1610612736 | bytes 8126464 | tf_op jit(solution)/shard_map/dot_general | solution.py:11
  196.3 8.8 %all_gather.10 = bf16[8,192,256]{2,0,1:T(8,128)(2,1)S(1)} all-gather(bf16[8,48,256]{2,0,1:T(8,128)(2,1)S(1)} %copy.25), channel_id=1, replica_groups=mesh['sp'=8,'tp'=4] {'tp'}, dimensions={1}, use_global_device_ids=true | all-gather | bytes 983040 | tf_op jit(solution)/shard_map/all_gather | solution.py:187
  206.2 2.5 %fusion.10 = f32[256,256]{1,0:T(8,128)} fusion(bf16[1536,256]{1,0:T(8,128)(2,1)} %bitcast.63, bf16[1536,512]{1,0:T(8,128)(2,1)} %all-gather.2.cloned.1.call-done), kind=kOutput, calls=%fused_computation.28 | convolution fusion | flops 201326592 | bytes 1835008 | tf_op jit(solution)/shard_map/dot_general | solution.py:11
  (88 shorter events, 43.0 us)
Async XLA Ops:
  7.2 79.2 %copy-start = (bf16[1,2048,512]{2,1,0:T(8,128)(2,1)S(1)}, bf16[1,2048,512]{2,1,0:T(8,128)(2,1)}, u32[]{:S(2)}) copy-start(bf16[1,2048,512]{2,1,0:T(8,128)(2,1)} %param.21) | copy-start | bytes 6291460
  7.2 11.4 %copy-start.10 = (f32[192,2]{0,1:T(2,128)S(1)}, f32[192,2]{0,1:T(2,128)}, u32[]{:S(2)}) copy-start(f32[192,2]{0,1:T(2,128)} %param.15) | copy-start | bytes 4612
  11.3 27.6 %all-to-all-start = ((bf16[8,96,512]{2,1,0:T(8,128)(2,1)}), bf16[8,96,512]{2,1,0:T(8,128)(2,1)}, u32[]{:S(2)}, u32[]{:S(2)}) async-start(bf16[8,96,512]{2,1,0:T(8,128)(2,1)} %bitcast.7), calls=%async_computation | async-start | bytes 1572864 | tf_op jit(solution)/shard_map/all_to_all | solution.py:130
  18.6 25.4 %copy-start.7 = (bf16[192,256]{1,0:T(8,128)(2,1)S(1)}, bf16[192,256]{1,0:T(8,128)(2,1)}, u32[]{:S(2)}) copy-start(bf16[192,256]{1,0:T(8,128)(2,1)} %param.18) | copy-start | bytes 294916
  18.6 25.4 %copy-start.8 = (bf16[192,256]{1,0:T(8,128)(2,1)S(1)}, bf16[192,256]{1,0:T(8,128)(2,1)}, u32[]{:S(2)}) copy-start(bf16[192,256]{1,0:T(8,128)(2,1)} %param.17) | copy-start | bytes 294916
  18.8 38.3 %copy-start.6 = (bf16[192,256]{1,0:T(8,128)(2,1)S(1)}, bf16[192,256]{1,0:T(8,128)(2,1)}, u32[]{:S(2)}) copy-start(bf16[192,256]{1,0:T(8,128)(2,1)} %param.16) | copy-start | bytes 294916
  38.9 18.2 %collective-permute-start.1 = (bf16[768,512]{1,0:T(8,128)(2,1)}, bf16[768,512]{1,0:T(8,128)(2,1)}, u32[]{:S(2)}, u32[]{:S(2)}) collective-permute-start(bf16[768,512]{1,0:T(8,128)(2,1)} %bitcast.11), channel_id=1, source_target_pairs={{0,2},{1,3},{2,0},{3,1},{4,6},{5,7},{6,4},{7,5},{8,10},{9,11},{10,... | collective-permute-start | bytes 2359304 | tf_op jit(solution)/shard_map/ppermute | solution.py:66
  40.4 26.0 %all-to-all-start.1 = ((bf16[8,96,512]{2,1,0:T(8,128)(2,1)}), bf16[8,96,512]{2,1,0:T(8,128)(2,1)S(1)}, u32[]{:S(2)}, u32[]{:S(2)}) async-start(bf16[8,96,512]{2,1,0:T(8,128)(2,1)} %bitcast.62), calls=%async_computation.1 | async-start | bytes 1572864 | tf_op jit(solution)/shard_map/all_to_all | solution.py:130
  44.0 18.1 %collective-permute-start = (bf16[768,512]{1,0:T(8,128)(2,1)}, bf16[768,512]{1,0:T(8,128)(2,1)}, u32[]{:S(2)}, u32[]{:S(2)}) collective-permute-start(bf16[768,512]{1,0:T(8,128)(2,1)} %bitcast.11), channel_id=1, source_target_pairs={{0,1},{1,0},{2,3},{3,2},{4,5},{5,4},{6,7},{7,6},{8,9},{9,8},{10,11... | collective-permute-start | bytes 2359304 | tf_op jit(solution)/shard_map/ppermute | solution.py:67
  44.1 13.0 %collective-permute-start.6 = (f32[1,256]{1,0:T(1,128)S(1)}, f32[1,256]{1,0:T(1,128)S(1)}, u32[]{:S(2)}, u32[]{:S(2)}) collective-permute-start(f32[1,256]{1,0:T(1,128)S(1)} %get-tuple-element.28), channel_id=1, source_target_pairs={{0,4},{4,8},{8,12},{12,16},{16,20},{20,24},{24,28},{1,5},{5,9},{9,... | collective-permute-start | bytes 3080 | tf_op jit(solution)/shard_map/ppermute | solution.py:25
  48.0 9.1 %collective-permute-start.7 = (f32[1,256]{1,0:T(1,128)S(1)}, f32[1,256]{1,0:T(1,128)S(1)}, u32[]{:S(2)}, u32[]{:S(2)}) collective-permute-start(f32[1,256]{1,0:T(1,128)S(1)} %get-tuple-element.29), channel_id=1, source_target_pairs={{4,0},{8,4},{12,8},{16,12},{20,16},{24,20},{28,24},{5,1},{9,5},{13... | collective-permute-start | bytes 3080 | tf_op jit(solution)/shard_map/ppermute | solution.py:26
  57.1 11.9 %collective-permute-start.2 = (bf16[768,512]{1,0:T(8,128)(2,1)}, bf16[768,512]{1,0:T(8,128)(2,1)}, u32[]{:S(2)}, u32[]{:S(2)}) collective-permute-start(bf16[768,512]{1,0:T(8,128)(2,1)} %collective-permute-done.1), channel_id=1, source_target_pairs={{0,1},{1,0},{2,3},{3,2},{4,5},{5,4},{6,7},{7,6},{8,9},{9,8},{10,11... | collective-permute-start | bytes 2359304 | tf_op jit(solution)/shard_map/ppermute | solution.py:67
  66.4 23.7 %collective-permute-start.3 = (bf16[768,512]{1,0:T(8,128)(2,1)S(1)}, bf16[768,512]{1,0:T(8,128)(2,1)S(1)}, u32[]{:S(2)}, u32[]{:S(2)}) collective-permute-start(bf16[768,512]{1,0:T(8,128)(2,1)S(1)} %bitcast.59), channel_id=1, source_target_pairs={{0,1},{1,0},{2,3},{3,2},{4,5},{5,4},{6,7},{7,6},{8,9},{9,8},{10,11... | collective-permute-start | bytes 2359304 | tf_op jit(solution)/shard_map/ppermute | solution.py:67
  66.9 19.4 %collective-permute-start.4 = (bf16[768,512]{1,0:T(8,128)(2,1)S(1)}, bf16[768,512]{1,0:T(8,128)(2,1)S(1)}, u32[]{:S(2)}, u32[]{:S(2)}) collective-permute-start(bf16[768,512]{1,0:T(8,128)(2,1)S(1)} %bitcast.60), channel_id=1, source_target_pairs={{0,2},{1,3},{2,0},{3,1},{4,6},{5,7},{6,4},{7,5},{8,10},{9,11},{10,... | collective-permute-start | bytes 2359304 | tf_op jit(solution)/shard_map/ppermute | solution.py:66
  75.0 15.4 %copy-start.12 = (f32[768,512]{1,0:T(8,128)}, f32[768,512]{1,0:T(8,128)S(1)}, u32[]{:S(2)}) copy-start(f32[768,512]{1,0:T(8,128)S(1)} %fusion.1) | copy-start | bytes 4718596
  86.4 3.9 %collective-permute-start.5 = (bf16[768,512]{1,0:T(8,128)(2,1)S(1)}, bf16[768,512]{1,0:T(8,128)(2,1)S(1)}, u32[]{:S(2)}, u32[]{:S(2)}) collective-permute-start(bf16[768,512]{1,0:T(8,128)(2,1)S(1)} %collective-permute-done.4), channel_id=1, source_target_pairs={{0,1},{1,0},{2,3},{3,2},{4,5},{5,4},{6,7},{7,6},{8,9},{9,8},{10,11... | collective-permute-start | bytes 2359304 | tf_op jit(solution)/shard_map/ppermute | solution.py:67
  102.9 2.8 %collective-permute-start.9 = (bf16[768,512]{1,0:T(8,128)(2,1)}, bf16[768,512]{1,0:T(8,128)(2,1)}, u32[]{:S(2)}, u32[]{:S(2)}) collective-permute-start(bf16[768,512]{1,0:T(8,128)(2,1)} %get-tuple-element.19), channel_id=1, source_target_pairs={{0,1},{1,0},{2,3},{3,2},{4,5},{5,4},{6,7},{7,6},{8,9},{9,8},{10,11... | collective-permute-start | bytes 2359304 | tf_op jit(solution)/shard_map/ppermute | solution.py:46
  103.4 6.6 %collective-permute-start.8 = (bf16[768,512]{1,0:T(8,128)(2,1)}, bf16[768,512]{1,0:T(8,128)(2,1)}, u32[]{:S(2)}, u32[]{:S(2)}) collective-permute-start(bf16[768,512]{1,0:T(8,128)(2,1)} %get-tuple-element.18), channel_id=1, source_target_pairs={{0,1},{1,0},{2,3},{3,2},{4,5},{5,4},{6,7},{7,6},{8,9},{9,8},{10,11... | collective-permute-start | bytes 2359304 | tf_op jit(solution)/shard_map/ppermute | solution.py:46
  108.5 20.1 %collective-permute-start.10 = (bf16[768,512]{1,0:T(8,128)(2,1)}, bf16[768,512]{1,0:T(8,128)(2,1)}, u32[]{:S(2)}, u32[]{:S(2)}) collective-permute-start(bf16[768,512]{1,0:T(8,128)(2,1)} %add_convert_fusion.1), channel_id=1, source_target_pairs={{0,2},{1,3},{2,0},{3,1},{4,6},{5,7},{6,4},{7,5},{8,10},{9,11},{10,... | collective-permute-start | bytes 2359304 | tf_op jit(solution)/shard_map/ppermute | solution.py:51
  131.7 35.0 %all-to-all-start.2 = ((bf16[8,96,512]{2,1,0:T(8,128)(2,1)}), bf16[8,96,512]{2,1,0:T(8,128)(2,1)}, u32[]{:S(2)}, u32[]{:S(2)}) async-start(bf16[8,96,512]{2,1,0:T(8,128)(2,1)} %bitcast.23), calls=%async_computation.2 | async-start | bytes 1572864 | tf_op jit(solution)/shard_map/all_to_all | solution.py:130
  141.4 64.8 %all-gather.2.cloned.1.call-start = ((), (), s32[]{:S(2)}) async-start(), calls=%async_computation.4 | async-start | bytes 1769472 | tf_op jit(solution)/shard_map/all_gather | solution.py:156
  178.1 16.2 %collective-permute-start.11 = (f32[1,256]{1,0:T(1,128)S(1)}, f32[1,256]{1,0:T(1,128)S(1)}, u32[]{:S(2)}, u32[]{:S(2)}) collective-permute-start(f32[1,256]{1,0:T(1,128)S(1)} %get-tuple-element.24), channel_id=1, source_target_pairs={{4,0},{8,4},{12,8},{16,12},{20,16},{24,20},{28,24},{5,1},{9,5},{13... | collective-permute-start | bytes 3080 | tf_op jit(solution)/shard_map/ppermute | solution.py:26
  179.4 14.9 %collective-permute-start.12 = (f32[1,256]{1,0:T(1,128)S(1)}, f32[1,256]{1,0:T(1,128)S(1)}, u32[]{:S(2)}, u32[]{:S(2)}) collective-permute-start(f32[1,256]{1,0:T(1,128)S(1)} %get-tuple-element.25), channel_id=1, source_target_pairs={{0,4},{4,8},{8,12},{12,16},{16,20},{20,24},{24,28},{1,5},{5,9},{9,... | collective-permute-start | bytes 3080 | tf_op jit(solution)/shard_map/ppermute | solution.py:25
  184.7 11.5 %all-to-all-start.3 = ((bf16[8,48,256]{2,1,0:T(8,128)(2,1)}), bf16[8,48,256]{2,1,0:T(8,128)(2,1)S(1)}, u32[]{:S(2)}, u32[]{:S(2)}) async-start(bf16[8,48,256]{2,1,0:T(8,128)(2,1)} %copy.24), calls=%async_computation.3 | async-start | bytes 393216 | tf_op jit(solution)/shard_map/all_to_all | solution.py:184
  (8 other events, 24.1 us)
Sparse Core Ops, SparseCore 0:
  144.4 46.1 all-gather.1
where the time goes:
time: 217 us; the launch traced here: 216 us
  waiting for transfers between devices  70.4 us (32%)
  matrix products  42.5 us (20%)
  starting transfers between devices  41.2 us (19%)
  local copies, waits for them, and re-layouts  21.8 us (10%)
  blocking collectives  16.9 us (8%)
  between operations  14.5 us (7%)
  other arithmetic  8.44 us (4%)
    all_to_all x3, waiting for transfers between devices, dispatched(): return lax.all_to_all(rows, 'sp', split_axis=0, concat_axis=0, tiled=True)  29.6 us
    dot_general x5, matrix products, contract_rows(): lax.dot_general(left, right, (((0,), (0,)), ((), ())), preferred_element_...  22.6 us
    all_to_all x3, starting transfers between devices, dispatched(): return lax.all_to_all(rows, 'sp', split_axis=0, concat_axis=0, tiled=True)  20.5 us
    ppermute x1, waiting for transfers between devices, exchange_groups(): got = lax.ppermute(sums[step - 1].astype(jnp.bfloat16), 'tp', moves)  18.6 us
    ppermute x2, waiting for transfers between devices, gather_features(): held.append(lax.ppermute(part, 'tp', moves))  18.2 us
    all_gather x1, blocking collectives, local(): features = lax.all_gather(quarter, 'tp', axis=1, tiled=True)  8.84 us
    ppermute x2, starting transfers between devices, halo(): lax.ppermute(cells[-1:], axis, [(i, (i + 1) % count) for i in range(ends)])  8.46 us
    all_gather x1, blocking collectives, local(): residual = lax.all_gather(token_grad, 'tp', axis=1, tiled=True)  8.05 us
  transfers between devices with their start and end apart: 18, of which 7 were waited for; matrix products, arithmetic and copies ran while one was open for 23% of the time, Pallas kernels for 0%

commit v1 on v0

--- a/solution.py
+++ b/solution.py
@@ -1,10 +1,586 @@
+import functools
+import math
+
 import jax
 import jax.numpy as jnp
 from jax import lax
+from jax.experimental import pallas as pl
+from jax.experimental.pallas import tpu as pltpu
 from jax.sharding import PartitionSpec as P
 
 CLAMP_LIMIT = 7.0
 SILU_ALPHA = 1.702
+MESH = pl.DeviceIdType.MESH
+BF16 = jnp.bfloat16
+F32 = jnp.float32
+
+
+def dot(left, right, dims):
+    return lax.dot_general(left, right, (dims, ((), ())), preferred_element_type=F32)
+
+
+def rows_dot(left, right):
+    return dot(left, right, ((1,), (0,)))
+
+
+def cols_dot(left, right):
+    return dot(left, right, ((1,), (1,)))
+
+
+def outer_dot(left, right):
+    return dot(left, right, ((0,), (0,)))
+
+
+def neighbours_along(count):
+    side = math.isqrt(max(count // 2, 1))
+    return side if side and count % side == 0 else 1
+
+
+def exchange_kernel(
+    dims,
+    routes_ref, weights_ref, tokens_ref, cot_ref, gate_ref, conv_ref, value_ref, taps_ref,
+    outw_hbm, wg_hbm, wu_hbm, wd_hbm,
+    x_ref, hid_ref, dg_ref, du_ref, owg_ref, tg_ref, gg_ref, cg_ref, vg_ref,
+    tokq, cotq, wg, wu, wd, outw, place, sendb, psend, pown, precv, ysend, yrecv, share, comb,
+    tga, prod, halo_p, back, halo_b, conv_s, mixed, feat,
+    a_send, a_recv, y_send, y_recv, k_send, k_recv, p_send, p_recv, q_send, q_recv,
+    r_send, r_recv, ty_send, ty_recv, tk_send, tk_recv, h_send, h_recv, m_send, m_recv,
+    o_send, o_recv, oy_send, oy_recv, ok_send, ok_recv, l_sem,
+):
+    n_sp, n_tp, nx, cap, quarter, tok, width, chan, fh = dims
+    ny = n_tp // 2
+    groups = n_sp // nx
+    rows = nx * cap
+    chunk = width // n_sp
+    part = tok // n_tp
+    sp, tp = lax.axis_index("sp"), lax.axis_index("tp")
+    z, x = sp // nx, sp % nx
+    y, c = tp // 2, tp % 2
+    partner = (sp, y * 2 + 1 - c)
+
+    def tp_of(yy):
+        return yy * 2 + c
+
+    def y_peer(k):
+        return (y + k) % ny
+
+    def remote(src, dst, ssem, rsem, dev):
+        return pltpu.make_async_remote_copy(
+            src_ref=src, dst_ref=dst, send_sem=ssem, recv_sem=rsem,
+            device_id=dev, device_id_type=MESH,
+        )
+
+    barrier = pltpu.get_barrier_semaphore()
+
+    def greet(n, carry):
+        pl.semaphore_signal(barrier, inc=1, device_id=((sp + n) % n_sp, tp), device_id_type=MESH)
+        return carry
+
+    lax.fori_loop(1, n_sp, greet, 0)
+    for k in range(1, ny):
+        pl.semaphore_signal(barrier, inc=1, device_id=(sp, tp_of(y_peer(k))), device_id_type=MESH)
+    pl.semaphore_signal(barrier, inc=1, device_id=partner, device_id_type=MESH)
+
+    offset = pl.multiple_of(tp * quarter, quarter)
+    loads = [
+        pltpu.make_async_copy(tokens_ref.at[:, pl.ds(offset, quarter)], tokq, l_sem.at[0]),
+        pltpu.make_async_copy(cot_ref.at[:, pl.ds(offset, quarter)], cotq, l_sem.at[1]),
+        pltpu.make_async_copy(wg_hbm.at[0], wg, l_sem.at[2]),
+        pltpu.make_async_copy(wu_hbm.at[0], wu, l_sem.at[3]),
+        pltpu.make_async_copy(wd_hbm.at[0], wd, l_sem.at[4]),
+        pltpu.make_async_copy(outw_hbm, outw, l_sem.at[5]),
+    ]
+    for load in loads:
+        load.start()
+
+    experts = lax.broadcasted_iota(jnp.int32, (n_sp, tok), 0)
+    first, second = routes_ref[0:1, :], routes_ref[1:2, :]
+    hit_a, hit_b = experts == first, experts == second
+    hits = jnp.where(hit_a, 1.0, 0.0) + jnp.where(hit_b, 1.0, 0.0)
+    earlier = (
+        lax.broadcasted_iota(jnp.int32, (tok, tok), 0) < lax.broadcasted_iota(jnp.int32, (tok, tok), 1)
+    )
+    before = rows_dot(hits.astype(BF16), jnp.where(earlier, 1.0, 0.0).astype(BF16))
+
+    def slot_of(hit, named):
+        rank = jnp.sum(jnp.where(hit, before, 0.0), axis=0, keepdims=True).astype(jnp.int32)
+        return named * cap + rank
+
+    slot_a, slot_b = slot_of(hit_a, first), slot_of(hit_b, second)
+    weight_a, weight_b = weights_ref[0:1, :], weights_ref[1:2, :]
+    slot_iota = lax.broadcasted_iota(jnp.int32, (cap, tok), 0)
+
+    loads[0].wait()
+    loads[1].wait()
+    pl.semaphore_wait(barrier, (n_sp - 1) + (ny - 1) + 1)
+
+    def dispatch(n, carry):
+        d = ((z + n // nx) % groups) * nx + (x + n % nx) % nx
+        here_a = slot_iota + d * cap == slot_a
+        here_b = slot_iota + d * cap == slot_b
+        picked = jnp.where(here_a, 1.0, jnp.where(here_b, 1.0, 0.0)).astype(BF16)
+        scale = jnp.sum(
+            jnp.where(here_a, weight_a, jnp.where(here_b, weight_b, 0.0)), axis=1, keepdims=True
+        )
+        place[d] = picked
+        sendb[d, 0] = rows_dot(picked, tokq[...]).astype(BF16)
+        sendb[d, 1] = (rows_dot(picked, cotq[...]) * scale).astype(BF16)
+
+        @pl.when(d == sp)
+        def _():
+            x_ref[tp, sp] = sendb[d]
+
+        @pl.when(d != sp)
+        def _():
+            remote(sendb.at[d], x_ref.at[tp, sp], a_send.at[d], a_recv.at[sp], (d, tp)).start()
+
+        return carry
+
+    lax.fori_loop(0, n_sp, dispatch, 0)
+
+    gate_f = gate_ref[...].astype(F32)
+    conv_f = conv_ref[...].astype(F32)
+    value_f = value_ref[...].astype(F32)
+    prod[...] = conv_f * value_f
+    up_dev, down_dev = ((sp + 1) % n_sp, tp), ((sp + n_sp - 1) % n_sp, tp)
+
+    def halo_copies(source, landing, which):
+        to_next = remote(
+            source.at[pl.ds(tok - 8, 8)], landing.at[0], h_send.at[which, 0], h_recv.at[which, 0], up_dev
+        )
+        to_prev = remote(
+            source.at[pl.ds(0, 8)], landing.at[1], h_send.at[which, 1], h_recv.at[which, 1], down_dev
+        )
+        return to_next, to_prev
+
+    def halo_start(source, landing, which):
+        to_next, to_prev = halo_copies(source, landing, which)
+
+        @pl.when(sp < n_sp - 1)
+        def _():
+            to_next.start()
+
+        @pl.when(sp == n_sp - 1)
+        def _():
+            landing[1] = jnp.zeros(landing.shape[1:], F32)
+
+        @pl.when(sp > 0)
+        def _():
+            to_prev.start()
+
+        @pl.when(sp == 0)
+        def _():
+            landing[0] = jnp.zeros(landing.shape[1:], F32)
+
+    def halo_finish(source, landing, which):
+        to_next, to_prev = halo_copies(source, landing, which)
+
+        @pl.when(sp < n_sp - 1)
+        def _():
+            to_next.wait_send()
+            to_prev.wait_recv()
+
+        @pl.when(sp > 0)
+        def _():
+            to_prev.wait_send()
+            to_next.wait_recv()
+
+    def shifted(cells, landing):
+        at_row = lax.broadcasted_iota(jnp.int32, cells.shape, 0)
+        above = jnp.where(at_row == 0, landing[0, 7:8, :], pltpu.roll(cells, 1, 0))
+        below = jnp.where(at_row == tok - 1, landing[1, 0:1, :], pltpu.roll(cells, tok - 1, 0))
+        return above, below
+
+    halo_start(prod, halo_p, 0)
+    tap_at = pl.ds(pl.multiple_of(tp * chan, chan), chan)
+    tap0, tap1, tap2 = taps_ref[0:1, tap_at], taps_ref[1:2, tap_at], taps_ref[2:3, tap_at]
+
+    def group_of(i):
+        return (z + groups - i) % groups
+
+    def arrive(i):
+        for j in range(nx):
+            s = group_of(i) * nx + (x + nx - j) % nx
+
+            @pl.when(s != sp)
+            def _():
+                remote(
+                    x_ref.at[tp, s], x_ref.at[tp, s], a_send.at[s], a_recv.at[s], (s, tp)
+                ).wait_recv()
+
+            for k in range(1, ny):
+                yy = y_peer(k)
+                remote(
+                    x_ref.at[tp, s], x_ref.at[tp, s], y_send.at[yy, s], y_recv.at[y, s], (sp, tp_of(yy))
+                ).start()
+            remote(
+                x_ref.at[tp, s], x_ref.at[tp, s], k_send.at[y, s], k_recv.at[y, s], partner
+            ).start()
+
+    def relay(i):
+        for j in range(nx):
+            s = group_of(i) * nx + (x + nx - j) % nx
+            for k in range(1, ny):
+                yy = y_peer(k)
+                landed = x_ref.at[tp_of(yy), s]
+                remote(landed, landed, y_send.at[yy, s], y_recv.at[yy, s], (sp, tp_of(yy))).wait_recv()
+                remote(landed, landed, k_send.at[yy, s], k_recv.at[yy, s], partner).start()
+
+    def compute(i):
+        g = group_of(i)
+        s0 = g * nx
+        for j in range(nx):
+            for yy in range(ny):
+                landed = x_ref.at[yy * 2 + 1 - c, s0 + j]
+                remote(landed, landed, k_send.at[yy, s0 + j], k_recv.at[yy, s0 + j], partner).wait_recv()
+        gate_pre = jnp.zeros((rows, fh), F32)
+        up_pre = jnp.zeros((rows, fh), F32)
+        d_hidden = jnp.zeros((rows, fh), F32)
+        for q in range(n_tp):
+            cells = x_ref[q, pl.ds(s0, nx), 0].reshape(rows, quarter)
+            gate_pre += rows_dot(cells, wg[q * quarter:(q + 1) * quarter, :])
+            up_pre += rows_dot(cells, wu[q * quarter:(q + 1) * quarter, :])
+        for q in range(n_tp):
+            cells = x_ref[q, pl.ds(s0, nx), 1].reshape(rows, quarter)
+            d_hidden += cols_dot(cells, wd[:, q * quarter:(q + 1) * quarter])
+        gate_clip = jnp.minimum(gate_pre, CLAMP_LIMIT)
+        up_clip = jnp.clip(up_pre, -CLAMP_LIMIT, CLAMP_LIMIT)
+        sig = jax.nn.sigmoid(SILU_ALPHA * gate_clip)
+        act = gate_clip * sig
+        mine = pl.ds(pl.multiple_of(g * rows, rows), rows)
+        hid_ref[mine, :] = ((up_clip + 1.0) * act).astype(BF16)
+        d_up = jnp.where(jnp.abs(up_pre) < CLAMP_LIMIT, d_hidden * act, 0.0).astype(BF16)
+        slope = sig + SILU_ALPHA * act * (1.0 - sig)
+        d_gate = jnp.where(gate_pre < CLAMP_LIMIT, d_hidden * (up_clip + 1.0) * slope, 0.0).astype(BF16)
+        dg_ref[mine, :] = d_gate
+        du_ref[mine, :] = d_up
+
+        def partial_of(q):
+            at = pl.ds(pl.multiple_of(q * quarter, quarter), quarter)
+            return cols_dot(d_gate, wg[at, :]) + cols_dot(d_up, wu[at, :])
+
+        for yy in range(ny):
+            psend[g, yy] = partial_of(yy * 2 + 1 - c).astype(BF16)
+        remote(psend.at[g], precv.at[g], p_send.at[g], p_recv.at[g], partner).start()
+        for yy in range(ny):
+            pown[g, yy] = partial_of(yy * 2 + c)
+
+    def reduce_cores(i):
+        g = group_of(i)
+        remote(psend.at[g], precv.at[g], p_send.at[g], p_recv.at[g], partner).wait_recv()
+        for k in range(1, ny):
+            yy = y_peer(k)
+            ysend[g, yy] = (pown[g, yy] + precv[g, yy].astype(F32)).astype(BF16)
+            remote(
+                ysend.at[g, yy], yrecv.at[g, y], q_send.at[yy, g], q_recv.at[y, g], (sp, tp_of(yy))
+            ).start()
+        pown[g, y] = pown[g, y] + precv[g, y].astype(F32)
+
+    def give_back(i):
+        g = group_of(i)
+        total = pown[g, y]
+        for k in range(1, ny):
+            yy = y_peer(k)
+            remote(
+                ysend.at[g, yy], yrecv.at[g, yy], q_send.at[yy, g], q_recv.at[yy, g], (sp, tp_of(yy))
+            ).wait_recv()
+            total = total + yrecv[g, yy].astype(F32)
+        share[pl.ds(g * nx, nx)] = total.astype(BF16).reshape(nx, cap, quarter)
+        for j in range(nx):
+            s = g * nx + (x + j) % nx
+
+            @pl.when(s != sp)
+            def _():
+                remote(share.at[s], comb.at[sp], r_send.at[s], r_recv.at[sp], (s, tp)).start()
+
+            @pl.when(s == sp)
+            def _():
+                comb[s] = share[s]
+
+    for load in loads[2:]:
+        load.wait()
+
+    def step(i, carry):
+        pl.when(i < groups)(lambda: arrive(i))
+        pl.when((i >= 2) & (i < groups + 2))(lambda: compute(i - 2))
+        pl.when((i >= 1) & (i < groups + 1))(lambda: relay(i - 1))
+        pl.when((i >= 2) & (i < groups + 2))(lambda: reduce_cores(i - 2))
+        pl.when(i >= 3)(lambda: give_back(i - 3))
+        return carry
+
+    lax.fori_loop(0, groups + 3, step, 0)
+
+    halo_finish(prod, halo_p, 0)
+    above, below = shifted(prod[...], halo_p)
+    conv_out = tap0 * above + tap1 * prod[...] + tap2 * below
+    conv_s[...] = conv_out
+    mixed[sp] = (gate_f * conv_out).astype(BF16)
+
+    def send_mixed(n, carry):
+        d = (sp + n) % n_sp
+        remote(mixed.at[sp], mixed.at[sp], m_send.at[d], m_recv.at[sp], (d, tp)).start()
+        return carry
+
+    lax.fori_loop(1, n_sp, send_mixed, 0)
+
+    tg_ref[...] = jnp.zeros_like(tg_ref)
+
+    def collect(n, acc):
+        d = ((z + n // nx) % groups) * nx + (x + n % nx) % nx
+
+        @pl.when(d != sp)
+        def _():
+            remote(share.at[d], comb.at[d], r_send.at[d], r_recv.at[d], (d, tp)).wait_recv()
+
+        return acc + outer_dot(place[d], comb[d])
+
+    acc = lax.fori_loop(0, n_sp, collect, cotq[...].astype(F32))
+    token_grad = acc.astype(BF16)
+    tg_ref[...] = token_grad
+    tga[tp] = token_grad
+
+    for k in range(1, ny):
+        yy = y_peer(k)
+        remote(tga.at[tp], tga.at[tp], ty_send.at[yy], ty_recv.at[y], (sp, tp_of(yy))).start()
+    remote(tga.at[tp], tga.at[tp], tk_send.at[y], tk_recv.at[y], partner).start()
+    for k in range(1, ny):
+        yy = y_peer(k)
+        landed = tga.at[tp_of(yy)]
+        remote(landed, landed, ty_send.at[yy], ty_recv.at[yy], (sp, tp_of(yy))).wait_recv()
+        remote(landed, landed, tk_send.at[yy], tk_recv.at[yy], partner).start()
+    for yy in range(ny):
+        landed = tga.at[yy * 2 + 1 - c]
+        remote(landed, landed, tk_send.at[yy], tk_recv.at[yy], partner).wait_recv()
+
+    def feature_of(d):
+        lane = (d * chunk) % quarter
+        return tga.at[
+            (d * chunk) // quarter,
+            pl.ds(pl.multiple_of(tp * part, part), part),
+            pl.ds(pl.multiple_of(lane, chunk), chunk),
+        ]
+
+    def send_features(n, carry):
+        d = (sp + n) % n_sp
+        remote(feature_of(d), feat.at[tp, sp], o_send.at[d], o_recv.at[sp], (d, tp)).start()
+        return carry
+
+    lax.fori_loop(1, n_sp, send_features, 0)
+    feat[tp, sp] = feature_of(sp)[...]
+
+    d_conv = jnp.zeros((tok, chan), F32)
+    for q in range(n_tp):
+        d_conv += rows_dot(tga[q], outw[q * quarter:(q + 1) * quarter, :])
+    back[...] = d_conv * gate_f
+    halo_start(back, halo_b, 1)
+    gg_ref[...] = (d_conv * conv_s[...]).astype(BF16)
+
+    halo_finish(back, halo_b, 1)
+    above, below = shifted(back[...], halo_b)
+    d_prod = tap0 * below + tap1 * back[...] + tap2 * above
+    cg_ref[...] = (d_prod * value_f).astype(BF16)
+    vg_ref[...] = (d_prod * conv_f).astype(BF16)
+
+    def land_features(n, carry):
+        s = (sp + n_sp - n) % n_sp
+        landed = feat.at[tp, s]
+        remote(feature_of(s), landed, o_send.at[s], o_recv.at[s], (s, tp)).wait_recv()
+        return carry
+
+    lax.fori_loop(1, n_sp, land_features, 0)
+    for k in range(1, ny):
+        yy = y_peer(k)
+        remote(feat.at[tp], feat.at[tp], oy_send.at[yy], oy_recv.at[y], (sp, tp_of(yy))).start()
+    remote(feat.at[tp], feat.at[tp], ok_send.at[y], ok_recv.at[y], partner).start()
+
+    def land_mixed(n, carry):
+        s = (sp + n_sp - n) % n_sp
+        remote(mixed.at[s], mixed.at[s], m_send.at[s], m_recv.at[s], (s, tp)).wait_recv()
+        return carry
+
+    lax.fori_loop(1, n_sp, land_mixed, 0)
+    for k in range(1, ny):
+        yy = y_peer(k)
+        landed = feat.at[tp_of(yy)]
+        remote(landed, landed, oy_send.at[yy], oy_recv.at[yy], (sp, tp_of(yy))).wait_recv()
+        remote(landed, landed, ok_send.at[yy], ok_recv.at[yy], partner).start()
+    for yy in range(ny):
+        landed = feat.at[yy * 2 + 1 - c]
+        remote(landed, landed, ok_send.at[yy], ok_recv.at[yy], partner).wait_recv()
+    owg = jnp.zeros((chunk, chan), F32)
+    for t in range(n_tp):
+        left = feat[t].reshape(n_sp * part, chunk)
+        right = mixed[:, t * part:(t + 1) * part, :].reshape(n_sp * part, chan)
+        owg += outer_dot(left, right)
+    owg_ref[...] = owg
+
+    def drain(n, carry):
+        d = (sp + n) % n_sp
+        remote(sendb.at[d], sendb.at[d], a_send.at[d], a_recv.at[d], (d, tp)).wait_send()
+        remote(share.at[d], share.at[d], r_send.at[d], r_recv.at[d], (d, tp)).wait_send()
+        remote(mixed.at[sp], mixed.at[sp], m_send.at[d], m_recv.at[d], (d, tp)).wait_send()
+        remote(feature_of(d), feat.at[tp, sp], o_send.at[d], o_recv.at[d], (d, tp)).wait_send()
+        return carry
+
+    lax.fori_loop(1, n_sp, drain, 0)
+
+    def drain_blocks(s, carry):
+        for k in range(1, ny):
+            yy = y_peer(k)
+            mine = x_ref.at[tp, s]
+            remote(mine, mine, y_send.at[yy, s], y_recv.at[yy, s], (sp, tp_of(yy))).wait_send()
+        for yy in range(ny):
+            mine = x_ref.at[tp_of(yy), s]
+            remote(mine, mine, k_send.at[yy, s], k_recv.at[yy, s], partner).wait_send()
+        return carry
+
+    lax.fori_loop(0, n_sp, drain_blocks, 0)
+
+    def drain_groups(g, carry):
+        remote(psend.at[g], precv.at[g], p_send.at[g], p_recv.at[g], partner).wait_send()
+        for k in range(1, ny):
+            yy = y_peer(k)
+            remote(
+                ysend.at[g, yy], yrecv.at[g, y], q_send.at[yy, g], q_recv.at[y, g], (sp, tp_of(yy))
+            ).wait_send()
+        return carry
+
+    lax.fori_loop(0, groups, drain_groups, 0)
+    for k in range(1, ny):
+        yy = y_peer(k)
+        remote(tga.at[tp], tga.at[tp], ty_send.at[yy], ty_recv.at[y], (sp, tp_of(yy))).wait_send()
+        remote(feat.at[tp], feat.at[tp], oy_send.at[yy], oy_recv.at[y], (sp, tp_of(yy))).wait_send()
+    for yy in range(ny):
+        mine = tga.at[tp_of(yy)]
+        remote(mine, mine, tk_send.at[yy], tk_recv.at[yy], partner).wait_send()
+        mine = feat.at[tp_of(yy)]
+        remote(mine, mine, ok_send.at[yy], ok_recv.at[yy], partner).wait_send()
+
+
+def grads_kernel(
+    x_ref, hid_ref, dg_ref, du_ref, owg_in, tg_in, gg_in, cg_in, vg_in,
+    gate_out, up_out, down_out, owg_out, tg_out, gg_out, cg_out, vg_out, hid_t,
+):
+    slots = hid_ref.shape[0]
+    quarter = x_ref.shape[-1]
+
+    @pl.when(pl.program_id(0) == 0)
+    def _():
+        hid_t[...] = hid_ref[...].T
+        owg_out[...] = owg_in[...]
+        tg_out[...] = tg_in[...]
+        gg_out[...] = gg_in[...]
+        cg_out[...] = cg_in[...]
+        vg_out[...] = vg_in[...]
+
+    rows = x_ref[0, :, 0].reshape(slots, quarter).T
+    grads = x_ref[0, :, 1].reshape(slots, quarter)
+    gate_out[0] = rows_dot(rows, dg_ref[...])
+    up_out[0] = rows_dot(rows, du_ref[...])
+    down_out[0] = rows_dot(hid_t[...], grads)
+
+
+def local_kernels(
+    saved_tokens, cotangent, routes, route_weights, gate_in, conv_in, value_in, conv_taps,
+    out_weight, gate_proj, up_proj, down_proj,
+):
+    tok, width = saved_tokens.shape
+    n_sp, n_tp = lax.axis_size("sp"), lax.axis_size("tp")
+    top = routes.shape[1]
+    cap = 2 * tok * top // n_sp
+    nx = neighbours_along(n_sp)
+    ny, groups = n_tp // 2, n_sp // nx
+    quarter = width // n_tp
+    chan = gate_in.shape[1]
+    fh = gate_proj.shape[2]
+    chunk, part = width // n_sp, tok // n_tp
+    rows = nx * cap
+    slots = n_sp * cap
+    dims = (n_sp, n_tp, nx, cap, quarter, tok, width, chan, fh)
+    vmem = pl.BlockSpec(memory_space=pltpu.VMEM)
+    hbm = pl.BlockSpec(memory_space=pl.ANY)
+    dma = pltpu.SemaphoreType.DMA
+    struct = jax.ShapeDtypeStruct
+    outs = pl.pallas_call(
+        functools.partial(exchange_kernel, dims),
+        name="exchange",
+        out_shape=(
+            struct((n_tp, n_sp, 2, cap, quarter), BF16),
+            struct((slots, fh), BF16),
+            struct((slots, fh), BF16),
+            struct((slots, fh), BF16),
+            struct((chunk, chan), F32),
+            struct((tok, quarter), BF16),
+            struct((tok, chan), BF16),
+            struct((tok, chan), BF16),
+            struct((tok, chan), BF16),
+        ),
+        in_specs=[vmem, vmem, hbm, hbm, vmem, vmem, vmem, vmem, hbm, hbm, hbm, hbm],
+        out_specs=(vmem,) * 9,
+        scratch_shapes=[
+            pltpu.VMEM((tok, quarter), BF16),
+            pltpu.VMEM((tok, quarter), BF16),
+            pltpu.VMEM((width, fh), BF16),
+            pltpu.VMEM((width, fh), BF16),
+            pltpu.VMEM((fh, width), BF16),
+            pltpu.VMEM((width, chan), BF16),
+            pltpu.VMEM((n_sp, cap, tok), BF16),
+            pltpu.VMEM((n_sp, 2, cap, quarter), BF16),
+            pltpu.VMEM((groups, ny, rows, quarter), BF16),
+            pltpu.VMEM((groups, ny, rows, quarter), F32),
+            pltpu.VMEM((groups, ny, rows, quarter), BF16),
+            pltpu.VMEM((groups, ny, rows, quarter), BF16),
+            pltpu.VMEM((groups, ny, rows, quarter), BF16),
+            pltpu.VMEM((n_sp, cap, quarter), BF16),
+            pltpu.VMEM((n_sp, cap, quarter), BF16),
+            pltpu.VMEM((n_tp, tok, quarter), BF16),
+            pltpu.VMEM((tok, chan), F32),
+            pltpu.VMEM((2, 8, chan), F32),
+            pltpu.VMEM((tok, chan), F32),
+            pltpu.VMEM((2, 8, chan), F32),
+            pltpu.VMEM((tok, chan), F32),
+            pltpu.VMEM((n_sp, tok, chan), BF16),
+            pltpu.VMEM((n_tp, n_sp, part, chunk), BF16),
+            dma((n_sp,)), dma((n_sp,)),
+            dma((ny, n_sp)), dma((ny, n_sp)),
+            dma((ny, n_sp)), dma((ny, n_sp)),
+            dma((groups,)), dma((groups,)),
+            dma((ny, groups)), dma((ny, groups)),
+            dma((n_sp,)), dma((n_sp,)),
+            dma((ny,)), dma((ny,)),
+            dma((ny,)), dma((ny,)),
+            dma((2, 2)), dma((2, 2)),
+            dma((n_sp,)), dma((n_sp,)),
+            dma((n_sp,)), dma((n_sp,)),
+            dma((ny,)), dma((ny,)),
+            dma((ny,)), dma((ny,)),
+            dma((6,)),
+        ],
+        compiler_params=pltpu.CompilerParams(collective_id=0, has_side_effects=True),
+    )(
+        routes.T, route_weights.T, saved_tokens, cotangent, gate_in, conv_in, value_in, conv_taps,
+        out_weight, gate_proj, up_proj, down_proj,
+    )
+    exchanged, small = outs[:4], outs[4:]
+    whole = [pl.BlockSpec(a.shape, lambda q, n=a.ndim: (0,) * n) for a in exchanged[1:]]
+    passed = [pl.BlockSpec(a.shape, lambda q, n=a.ndim: (0,) * n) for a in small]
+    return pl.pallas_call(
+        grads_kernel,
+        name="weight_grads",
+        grid=(n_tp,),
+        out_shape=(
+            struct((1, width, fh), F32),
+            struct((1, width, fh), F32),
+            struct((1, fh, width), F32),
+        ) + tuple(struct(a.shape, a.dtype) for a in small),
+        in_specs=[pl.BlockSpec((1,) + exchanged[0].shape[1:], lambda q: (q, 0, 0, 0, 0))] + whole + passed,
+        out_specs=[
+            pl.BlockSpec((1, quarter, fh), lambda q: (0, q, 0)),
+            pl.BlockSpec((1, quarter, fh), lambda q: (0, q, 0)),
+            pl.BlockSpec((1, fh, quarter), lambda q: (0, 0, q)),
+        ] + passed,
+        scratch_shapes=[pltpu.VMEM((fh, slots), BF16)],
+    )(*exchanged, *small)
 
 
 def contract_rows(left, right):
@@ -73,7 +649,7 @@
     return whole
 
 
-def local(
+def local_collectives(
     saved_tokens,
     cotangent,
     routes,
@@ -199,6 +775,21 @@
     )
 
 
+def local(*arrays):
+    tok, width = arrays[0].shape
+    n_sp, n_tp = lax.axis_size("sp"), lax.axis_size("tp")
+    cap = 2 * tok * arrays[2].shape[1] // n_sp
+    aligned = (
+        arrays[2].shape[1] == 2
+        and n_tp % 2 == 0
+        and cap % 16 == 0
+        and tok % (16 * n_tp) == 0
+        and width % (128 * n_sp) == 0
+        and (width // n_tp) % (width // n_sp) == 0
+    )
+    return (local_kernels if aligned else local_collectives)(*arrays)
+
+
 def solution(mesh):
     in_specs = (
         P("sp", None),

time: 217 us -> 127 us (0.59)
  Pallas kernels: 0 us -> 125 us
  waiting for transfers between devices: 70.4 us -> 0 us
  matrix products: 42.5 us -> 0 us
  starting transfers between devices: 41.2 us -> 0 us
  local copies, waits for them, and re-layouts: 21.8 us -> 0 us
  blocking collectives: 16.9 us -> 0 us
  between operations: 14.5 us -> 0.65 us
  other arithmetic: 8.44 us -> 0 us
    pallas_call x0 -> x2, Pallas kernels: none -> 125 us  [the longest x1 115 us: local_kernels(): pl.pallas_call(functools.partial(exchange_kernel, dims), name='exchange',...]
    dot_general x14 -> x0, matrix products: 42.5 us -> none  [the longest x5 22.6 us: contract_rows(): lax.dot_general(left, right, (((0,), (0,)), ((), ())), preferred_element_...]
    ppermute x13 -> x0, waiting for transfers between devices: 39 us -> none  [the longest x1 18.6 us: exchange_groups(): got = lax.ppermute(sums[step - 1].astype(jnp.bfloat16), 'tp', moves)]
    all_to_all x4 -> x0, waiting for transfers between devices: 30.8 us -> none  [the longest x3 29.6 us: dispatched(): return lax.all_to_all(rows, 'sp', split_axis=0, concat_axis=0, tiled=True)]
    all_to_all x4 -> x0, starting transfers between devices: 24.2 us -> none  [the longest x3 20.5 us: dispatched(): return lax.all_to_all(rows, 'sp', split_axis=0, concat_axis=0, tiled=True)]
    all_gather x2 -> x0, blocking collectives: 16.9 us -> none  [the longest x1 8.84 us: local(): features = lax.all_gather(quarter, 'tp', axis=1, tiled=True)]
    ppermute x13 -> x0, starting transfers between devices: 16.8 us -> none  [the longest x2 8.46 us: halo(): lax.ppermute(cells[-1:], axis, [(i, (i + 1) % count) for i in range(ends)])]
    dynamic_update_slice x8 -> x0, local copies, waits for them, and re-layouts: 9.13 us -> none  [the longest x4 4.62 us: gather_features(): lax.dynamic_update_slice_in_dim(whole, twins[step], (first + 1 - side) *...]
  transfers between devices with their start and end apart: 18 -> 0, of which waited for: 7 -> 0; matrix products, arithmetic and copies ran while one was open for 23% -> 0% of each run, Pallas kernels for 0% -> 0%
where the time goes in v1:
time: 127 us; the launch traced here: 126 us
  Pallas kernels  125 us (98%)
    pallas_call x1, Pallas kernels, local_kernels(): pl.pallas_call(functools.partial(exchange_kernel, dims), name='exchange',...  115 us
    pallas_call x1, Pallas kernels, local_kernels(): pl.pallas_call(grads_kernel, name='weight_grads', grid=(n_tp,), out_shape...  10.7 us

profile of v1, /device:TPU:0, one launch (start us, length us, event | category | flops | bytes accessed | tf_op | source)
XLA Modules:
  0.0 126.1 jit_solution(10249278141508405920)
XLA Ops:
  0.6 114.8 %exchange.1 = (bf16[4,8,2,96,512]{4,3,2,1,0:T(8,128)(2,1)}, bf16[768,512]{1,0:T(8,128)(2,1)}, bf16[768,512]{1,0:T(8,128)(2,1)}, bf16[768,512]{1,0:T(8,128)(2,1)}...) custom-call(s32[2,192]{1,0:T(2,128)} %bitcast.2, ...), custom_call_target="tpu_custom_call" | custom-call | tf_op jit(solution)/shard_map/exchange/pallas_call | solution.py:504
  115.4 10.7 %weight_grads.1 = (f32[1,2048,512]{2,1,0:T(8,128)}, f32[1,2048,512]{2,1,0:T(8,128)}, f32[1,512,2048]{2,1,0:T(8,128)}, f32[256,256]{1,0:T(8,128)}, bf16[192,512]{...) custom-call(bf16[4,8,2,96,512]{4,3,2,1,0:T(8,128)(2,1)} %get-tuple-element.17.x_ref,, ...), custom_call_target="tpu_custom_call" | custom-call | tf_op jit(solution)/shard_map/weight_grads/pallas_call | solution.py:567

commit v2 on v0

--- a/solution.py
+++ b/solution.py
@@ -1,10 +1,640 @@
+import functools
+
 import jax
 import jax.numpy as jnp
 from jax import lax
+from jax.experimental import pallas as pl
+from jax.experimental.pallas import tpu as pltpu
 from jax.sharding import PartitionSpec as P
 
 CLAMP_LIMIT = 7.0
 SILU_ALPHA = 1.702
+AHEAD = 2
+MESH = pl.DeviceIdType.MESH
+BF16 = jnp.bfloat16
+F32 = jnp.float32
+
+
+def dot(left, right, dims):
+    return lax.dot_general(left, right, (dims, ((), ())), preferred_element_type=F32)
+
+
+def rows_dot(left, right):
+    return dot(left, right, ((1,), (0,)))
+
+
+def cols_dot(left, right):
+    return dot(left, right, ((1,), (1,)))
+
+
+def outer_dot(left, right):
+    return dot(left, right, ((0,), (0,)))
+
+
+def exchange_kernel(
+    dims,
+    routes_hbm, weights_hbm, tokens_hbm, cot_hbm, gate_hbm, conv_hbm, value_hbm, taps_hbm,
+    outw_hbm, wg_hbm, wu_hbm, wd_hbm,
+    gate_out, up_out, down_out, owg_ref, tg_ref, gg_ref, cg_ref, vg_ref,
+    x_ref, hid_ref, dg_ref, du_ref, hid_t,
+    routes_ref, weights_ref, tokens_ref, cot_ref, gate_ref, conv_ref, value_ref, taps_ref,
+    wg, wu, wd, outw, place, sendb, psend, pown, precv, ysend, yrecv, share, comb,
+    tga, prod, halo_p, back, halo_b, conv_s, mixed, feat,
+    a_send, a_recv, y_send, y_recv, k_send, k_recv, p_send, p_recv, q_send, q_recv,
+    r_send, r_recv, ty_send, ty_recv, tk_send, tk_recv, h_send, h_recv, m_send, m_recv,
+    o_send, o_recv, ok_send, ok_recv, l_sem,
+):
+    n_sp, n_tp, cap, quarter, tok, width, chan, fh = dims
+    ny = n_tp // 2
+    half = n_sp // 2
+    slots = n_sp * cap
+    chunk = width // n_sp
+    part = tok // 2
+    sp, tp = lax.axis_index("sp"), lax.axis_index("tp")
+    side, pos = sp // half, sp % half
+    mirror = (1 - side) * half + pos
+    y, c = tp // 2, tp % 2
+    partner = (sp, y * 2 + 1 - c)
+
+    def near(r):
+        return side * half + (pos + half + r) % half
+
+    def far(r):
+        return (1 - side) * half + (pos + half + r) % half
+
+    def tp_of(yy):
+        return yy * 2 + c
+
+    def y_peer(k):
+        return (y + k) % ny
+
+    def remote(src, dst, ssem, rsem, dev):
+        return pltpu.make_async_remote_copy(
+            src_ref=src, dst_ref=dst, send_sem=ssem, recv_sem=rsem,
+            device_id=dev, device_id_type=MESH,
+        )
+
+    barrier = pltpu.get_barrier_semaphore()
+
+    def greet(n, carry):
+        pl.semaphore_signal(barrier, inc=1, device_id=((sp + n) % n_sp, tp), device_id_type=MESH)
+        return carry
+
+    lax.fori_loop(1, n_sp, greet, 0)
+    for k in range(1, ny):
+        pl.semaphore_signal(barrier, inc=1, device_id=(sp, tp_of(y_peer(k))), device_id_type=MESH)
+    pl.semaphore_signal(barrier, inc=1, device_id=partner, device_id_type=MESH)
+
+    sources = (
+        routes_hbm, weights_hbm, tokens_hbm, cot_hbm, gate_hbm, conv_hbm, value_hbm, taps_hbm,
+        wg_hbm.at[0], wu_hbm.at[0], wd_hbm.at[0], outw_hbm,
+    )
+    targets = (
+        routes_ref, weights_ref, tokens_ref, cot_ref, gate_ref, conv_ref, value_ref, taps_ref,
+        wg, wu, wd, outw,
+    )
+    loads = [
+        pltpu.make_async_copy(source, target, l_sem.at[n])
+        for n, (source, target) in enumerate(zip(sources, targets))
+    ]
+    early, late = loads[2:8], loads[8:]
+    for load in loads:
+        load.start()
+
+    loads[0].wait()
+    loads[1].wait()
+    experts = lax.broadcasted_iota(jnp.int32, (n_sp, tok), 0)
+    first, second = routes_ref[0:1, :], routes_ref[1:2, :]
+    hit_a, hit_b = experts == first, experts == second
+    hits = jnp.where(hit_a, 1.0, 0.0) + jnp.where(hit_b, 1.0, 0.0)
+    earlier = (
+        lax.broadcasted_iota(jnp.int32, (tok, tok), 0) < lax.broadcasted_iota(jnp.int32, (tok, tok), 1)
+    )
+    before = rows_dot(hits.astype(BF16), jnp.where(earlier, 1.0, 0.0).astype(BF16))
+
+    def slot_of(hit, named):
+        rank = jnp.sum(jnp.where(hit, before, 0.0), axis=0, keepdims=True).astype(jnp.int32)
+        return named * cap + rank
+
+    slot_a, slot_b = slot_of(hit_a, first), slot_of(hit_b, second)
+    weight_a, weight_b = weights_ref[0:1, :], weights_ref[1:2, :]
+    slot_iota = lax.broadcasted_iota(jnp.int32, (cap, tok), 0)
+    own = pl.ds(pl.multiple_of(tp * quarter, quarter), quarter)
+
+    def placed(d):
+        here_a = slot_iota + d * cap == slot_a
+        here_b = slot_iota + d * cap == slot_b
+        picked = jnp.where(here_a, 1.0, jnp.where(here_b, 1.0, 0.0)).astype(BF16)
+        scale = jnp.sum(
+            jnp.where(here_a, weight_a, jnp.where(here_b, weight_b, 0.0)), axis=1, keepdims=True
+        )
+        place[d] = picked
+        return picked, scale
+
+    def send_block(d):
+        picked, scale = placed(d)
+        sendb[d, 0] = rows_dot(picked, tokens_ref[:, own]).astype(BF16)
+        sendb[d, 1] = (rows_dot(picked, cot_ref[:, own]) * scale).astype(BF16)
+        remote(sendb.at[d], x_ref.at[tp, sp], a_send.at[d], a_recv.at[sp], (d, tp)).start()
+
+    for load in early:
+        load.wait()
+    gate_f = gate_ref[...].astype(F32)
+    conv_f = conv_ref[...].astype(F32)
+    value_f = value_ref[...].astype(F32)
+    prod[...] = conv_f * value_f
+    up_dev, down_dev = ((sp + 1) % n_sp, tp), ((sp + n_sp - 1) % n_sp, tp)
+
+    def halo_copies(source, landing, which):
+        to_next = remote(
+            source.at[pl.ds(tok - 8, 8)], landing.at[0], h_send.at[which, 0], h_recv.at[which, 0], up_dev
+        )
+        to_prev = remote(
+            source.at[pl.ds(0, 8)], landing.at[1], h_send.at[which, 1], h_recv.at[which, 1], down_dev
+        )
+        return to_next, to_prev
+
+    def halo_start(source, landing, which):
+        to_next, to_prev = halo_copies(source, landing, which)
+
+        @pl.when(sp < n_sp - 1)
+        def _():
+            to_next.start()
+
+        @pl.when(sp == n_sp - 1)
+        def _():
+            landing[1] = jnp.zeros(landing.shape[1:], F32)
+
+        @pl.when(sp > 0)
+        def _():
+            to_prev.start()
+
+        @pl.when(sp == 0)
+        def _():
+            landing[0] = jnp.zeros(landing.shape[1:], F32)
+
+    def halo_finish(source, landing, which):
+        to_next, to_prev = halo_copies(source, landing, which)
+
+        @pl.when(sp < n_sp - 1)
+        def _():
+            to_next.wait_send()
+            to_prev.wait_recv()
+
+        @pl.when(sp > 0)
+        def _():
+            to_prev.wait_send()
+            to_next.wait_recv()
+
+    def shifted(cells, landing):
+        at_row = lax.broadcasted_iota(jnp.int32, cells.shape, 0)
+        above = jnp.where(at_row == 0, landing[0, 7:8, :], pltpu.roll(cells, 1, 0))
+        below = jnp.where(at_row == tok - 1, landing[1, 0:1, :], pltpu.roll(cells, tok - 1, 0))
+        return above, below
+
+    pl.semaphore_wait(barrier, (n_sp - 1) + (ny - 1) + 1)
+    halo_start(prod, halo_p, 0)
+    tap_at = pl.ds(pl.multiple_of(tp * chan, chan), chan)
+    tap0, tap1, tap2 = taps_ref[0:1, tap_at], taps_ref[1:2, tap_at], taps_ref[2:3, tap_at]
+
+
+    def dispatch(r):
+        send_block(far(r))
+        pl.when(r + 1 < half)(lambda: send_block(near(r + 1)))
+
+    def dispatched(r):
+        d = far(r)
+        remote(sendb.at[d], sendb.at[d], a_send.at[d], a_recv.at[d], (d, tp)).wait_send()
+
+    for r in range(min(AHEAD, half)):
+        dispatch(r)
+
+    picked, scale = placed(sp)
+    for q in range(n_tp):
+        at = slice(q * quarter, (q + 1) * quarter)
+        x_ref[q, sp, 0] = rows_dot(picked, tokens_ref[:, at]).astype(BF16)
+        x_ref[q, sp, 1] = (rows_dot(picked, cot_ref[:, at]) * scale).astype(BF16)
+
+    halo_finish(prod, halo_p, 0)
+    above, below = shifted(prod[...], halo_p)
+    conv_out = tap0 * above + tap1 * prod[...] + tap2 * below
+    conv_s[...] = conv_out
+    mixed[sp] = (gate_f * conv_out).astype(BF16)
+
+    def mixed_copy(b, which, d):
+        return remote(mixed.at[b], mixed.at[b], m_send.at[which, d], m_recv.at[b], (d, tp))
+
+    mixed_copy(sp, 0, mirror).start()
+
+    def spread_own(r, carry):
+        mixed_copy(sp, 0, near(r)).start()
+        return carry
+
+    lax.fori_loop(1, half, spread_own, 0)
+
+    def spread_mirror():
+        mixed_copy(mirror, 0, mirror).wait_recv()
+
+        def one(r, carry):
+            mixed_copy(mirror, 1, near(r)).start()
+            return carry
+
+        lax.fori_loop(1, half, one, 0)
+
+    def land(s):
+        landed = x_ref.at[tp, s]
+        remote(landed, landed, a_send.at[s], a_recv.at[s], (s, tp)).wait_recv()
+        for k in range(1, ny):
+            yy = y_peer(k)
+            remote(landed, landed, y_send.at[yy, s], y_recv.at[y, s], (sp, tp_of(yy))).start()
+        remote(landed, landed, k_send.at[y, s], k_recv.at[y, s], partner).start()
+
+    def arrive(i):
+        dispatched(i)
+        pl.when(i + AHEAD < half)(lambda: dispatch(i + AHEAD))
+        pl.when(i + 1 < half)(lambda: land(near(-i - 1)))
+        land(far(-i))
+
+    def pass_on(s):
+        for k in range(1, ny):
+            yy = y_peer(k)
+            landed = x_ref.at[tp_of(yy), s]
+            remote(landed, landed, y_send.at[yy, s], y_recv.at[yy, s], (sp, tp_of(yy))).wait_recv()
+            remote(landed, landed, k_send.at[yy, s], k_recv.at[yy, s], partner).start()
+
+    def relay(i):
+        pl.when(i + 1 < half)(lambda: pass_on(near(-i - 1)))
+        pass_on(far(-i))
+
+    def complete(s):
+        for yy in range(ny):
+            landed = x_ref.at[yy * 2 + 1 - c, s]
+            remote(landed, landed, k_send.at[yy, s], k_recv.at[yy, s], partner).wait_recv()
+
+    def compute(i):
+        blocks = (near(-i), far(-i))
+        pl.when(i > 0)(lambda: complete(blocks[0]))
+        complete(blocks[1])
+
+        def cells(q, which):
+            return jnp.concatenate([x_ref[q, s, which] for s in blocks], axis=0)
+
+        rows = 2 * cap
+        gate_pre = jnp.zeros((rows, fh), F32)
+        up_pre = jnp.zeros((rows, fh), F32)
+        d_hidden = jnp.zeros((rows, fh), F32)
+        for q in range(n_tp):
+            gate_pre += rows_dot(cells(q, 0), wg[q * quarter:(q + 1) * quarter, :])
+            up_pre += rows_dot(cells(q, 0), wu[q * quarter:(q + 1) * quarter, :])
+        for q in range(n_tp):
+            d_hidden += cols_dot(cells(q, 1), wd[:, q * quarter:(q + 1) * quarter])
+        gate_clip = jnp.minimum(gate_pre, CLAMP_LIMIT)
+        up_clip = jnp.clip(up_pre, -CLAMP_LIMIT, CLAMP_LIMIT)
+        sig = jax.nn.sigmoid(SILU_ALPHA * gate_clip)
+        act = gate_clip * sig
+        hidden = ((up_clip + 1.0) * act).astype(BF16)
+        d_up = jnp.where(jnp.abs(up_pre) < CLAMP_LIMIT, d_hidden * act, 0.0).astype(BF16)
+        slope = sig + SILU_ALPHA * act * (1.0 - sig)
+        d_gate = jnp.where(gate_pre < CLAMP_LIMIT, d_hidden * (up_clip + 1.0) * slope, 0.0).astype(BF16)
+        for n, s in enumerate(blocks):
+            hid_ref[s] = hidden[n * cap:(n + 1) * cap]
+            dg_ref[s] = d_gate[n * cap:(n + 1) * cap]
+            du_ref[s] = d_up[n * cap:(n + 1) * cap]
+
+        def partial_of(q):
+            at = pl.ds(pl.multiple_of(q * quarter, quarter), quarter)
+            return cols_dot(d_gate, wg[at, :]) + cols_dot(d_up, wu[at, :])
+
+        for yy in range(ny):
+            psend[i, yy] = partial_of(yy * 2 + 1 - c).astype(BF16)
+        remote(psend.at[i], precv.at[i], p_send.at[i], p_recv.at[i], partner).start()
+        for yy in range(ny):
+            pown[i % 2, yy] = partial_of(yy * 2 + c)
+
+    def y_copy(i, n, yy, slot):
+        return remote(
+            ysend.at[i, n, yy], yrecv.at[i, n, slot], q_send.at[i, n, yy], q_recv.at[i, n, slot],
+            (sp, tp_of(yy)),
+        )
+
+    def reduce_cores(i):
+        remote(psend.at[i], precv.at[i], p_send.at[i], p_recv.at[i], partner).wait_recv()
+        for n in (1, 0):
+            at = slice(n * cap, (n + 1) * cap)
+            for k in range(1, ny):
+                yy = y_peer(k)
+                ysend[i, n, yy] = (pown[i % 2, yy, at] + precv[i, yy, at].astype(F32)).astype(BF16)
+                y_copy(i, n, yy, y).start()
+        pown[i % 2, y] = pown[i % 2, y] + precv[i, y].astype(F32)
+
+    def give_back(i):
+        for n, s in ((1, far(-i)), (0, near(-i))):
+            total = pown[i % 2, y, n * cap:(n + 1) * cap]
+            for k in range(1, ny):
+                yy = y_peer(k)
+                y_copy(i, n, yy, yy).wait_recv()
+                total = total + yrecv[i, n, yy].astype(F32)
+            share[s] = total.astype(BF16)
+            if n == 1:
+                remote(share.at[s], comb.at[sp], r_send.at[s], r_recv.at[sp], (s, tp)).start()
+            else:
+                @pl.when(i > 0)
+                def _():
+                    remote(share.at[s], comb.at[sp], r_send.at[s], r_recv.at[sp], (s, tp)).start()
+
+                @pl.when(i == 0)
+                def _():
+                    comb[sp] = share[sp]
+
+    def flat(ref):
+        return ref[...].reshape(slots, fh)
+
+    def input_grads(q):
+        left = x_ref[q, :, 0].reshape(slots, quarter).T
+        at = slice(q * quarter, (q + 1) * quarter)
+        gate_out[0, at, :] = rows_dot(left, flat(dg_ref))
+        up_out[0, at, :] = rows_dot(left, flat(du_ref))
+
+    def output_grads(q):
+        at = slice(q * quarter, (q + 1) * quarter)
+        down_out[0, :, at] = rows_dot(hid_t[...], x_ref[q, :, 1].reshape(slots, quarter))
+
+    for load in late:
+        load.wait()
+
+    def step(i, carry):
+        pl.when(i < half)(lambda: arrive(i))
+        pl.when((i >= 2) & (i < half + 2))(lambda: compute(i - 2))
+        pl.when((i >= 1) & (i < half + 1))(lambda: relay(i - 1))
+        pl.when((i >= 2) & (i < half + 2))(lambda: reduce_cores(i - 2))
+        pl.when(i == half)(spread_mirror)
+        pl.when(i >= 3)(lambda: give_back(i - 3))
+        return carry
+
+    lax.fori_loop(0, half + 2, step, 0)
+    hid_t[...] = flat(hid_ref).T
+    output_grads(0)
+    give_back(half - 1)
+    for q in range(1, n_tp):
+        output_grads(q)
+    input_grads(0)
+
+    def collect_from(d, acc):
+        @pl.when(d != sp)
+        def _():
+            remote(share.at[d], comb.at[d], r_send.at[d], r_recv.at[d], (d, tp)).wait_recv()
+
+        return acc + outer_dot(place[d], comb[d])
+
+    def collect(r, acc):
+        return collect_from(far(r), collect_from(near(r), acc))
+
+    acc = lax.fori_loop(0, half, collect, cot_ref[:, own].astype(F32))
+    token_grad = acc.astype(BF16)
+    tg_ref[...] = token_grad
+    tga[tp] = token_grad
+
+    for k in range(1, ny):
+        yy = y_peer(k)
+        remote(tga.at[tp], tga.at[tp], ty_send.at[yy], ty_recv.at[y], (sp, tp_of(yy))).start()
+    remote(tga.at[tp], tga.at[tp], tk_send.at[y], tk_recv.at[y], partner).start()
+    input_grads(1)
+    for k in range(1, ny):
+        yy = y_peer(k)
+        landed = tga.at[tp_of(yy)]
+        remote(landed, landed, ty_send.at[yy], ty_recv.at[yy], (sp, tp_of(yy))).wait_recv()
+        remote(landed, landed, tk_send.at[yy], tk_recv.at[yy], partner).start()
+    for yy in range(ny):
+        landed = tga.at[yy * 2 + 1 - c]
+        remote(landed, landed, tk_send.at[yy], tk_recv.at[yy], partner).wait_recv()
+
+    def feature_of(d):
+        lane = (d * chunk) % quarter
+        return tga.at[
+            (d * chunk) // quarter,
+            pl.ds(pl.multiple_of(c * part, part), part),
+            pl.ds(pl.multiple_of(lane, chunk), chunk),
+        ]
+
+    d_conv = jnp.zeros((tok, chan), F32)
+    for q in range(n_tp):
+        d_conv += rows_dot(tga[q], outw[q * quarter:(q + 1) * quarter, :])
+    back[...] = d_conv * gate_f
+    halo_start(back, halo_b, 1)
+
+    def send_features(r, carry):
+        d = far(r)
+        remote(feature_of(d), feat.at[c, sp], o_send.at[d], o_recv.at[sp], (d, tp)).start()
+
+        @pl.when(r > 0)
+        def _():
+            e = near(r)
+            remote(feature_of(e), feat.at[c, sp], o_send.at[e], o_recv.at[sp], (e, tp)).start()
+
+        return carry
+
+    lax.fori_loop(0, half, send_features, 0)
+    feat[c, sp] = feature_of(sp)[...]
+
+    gg_ref[...] = (d_conv * conv_s[...]).astype(BF16)
+    for q in range(2, n_tp):
+        input_grads(q)
+
+    halo_finish(back, halo_b, 1)
+    above, below = shifted(back[...], halo_b)
+    d_prod = tap0 * below + tap1 * back[...] + tap2 * above
+    cg_ref[...] = (d_prod * value_f).astype(BF16)
+    vg_ref[...] = (d_prod * conv_f).astype(BF16)
+
+    def land_features(r, carry):
+        def wait_from(s):
+            remote(feature_of(s), feat.at[c, s], o_send.at[s], o_recv.at[s], (s, tp)).wait_recv()
+
+        wait_from(far(-r))
+        pl.when(r > 0)(lambda: wait_from(near(-r)))
+        return carry
+
+    lax.fori_loop(0, half, land_features, 0)
+    feat_copy = remote(feat.at[c], feat.at[c], ok_send.at[0], ok_recv.at[0], partner)
+    feat_copy.start()
+
+    def land_mixed(n, carry):
+        s = (sp + n) % n_sp
+
+        @pl.when(s != mirror)
+        def _():
+            mixed_copy(s, 0, s).wait_recv()
+
+        return carry
+
+    lax.fori_loop(1, n_sp, land_mixed, 0)
+
+    def half_of(t):
+        left = feat[t].reshape(n_sp * part, chunk)
+        at = pl.ds(pl.multiple_of(t * part, part), part)
+        right = mixed[:, at, :].reshape(n_sp * part, chan)
+        return outer_dot(left, right)
+
+    owg = half_of(c)
+    feat_copy.wait_recv()
+    owg_ref[...] = owg + half_of(1 - c)
+
+    def drain(n, carry):
+        d = (sp + n) % n_sp
+        pl.when((d // half == side) & (d != sp))(
+            lambda: remote(sendb.at[d], sendb.at[d], a_send.at[d], a_recv.at[d], (d, tp)).wait_send()
+        )
+        remote(share.at[d], share.at[d], r_send.at[d], r_recv.at[d], (d, tp)).wait_send()
+        remote(feature_of(d), feat.at[c, sp], o_send.at[d], o_recv.at[d], (d, tp)).wait_send()
+        for k in range(1, ny):
+            yy = y_peer(k)
+            mine = x_ref.at[tp, d]
+            remote(mine, mine, y_send.at[yy, d], y_recv.at[yy, d], (sp, tp_of(yy))).wait_send()
+        for yy in range(ny):
+            mine = x_ref.at[tp_of(yy), d]
+            remote(mine, mine, k_send.at[yy, d], k_recv.at[yy, d], partner).wait_send()
+        return carry
+
+    lax.fori_loop(1, n_sp, drain, 0)
+    mixed_copy(sp, 0, mirror).wait_send()
+
+    def drain_rounds(i, carry):
+        remote(psend.at[i], precv.at[i], p_send.at[i], p_recv.at[i], partner).wait_send()
+        for n in (1, 0):
+            for k in range(1, ny):
+                y_copy(i, n, y_peer(k), y).wait_send()
+
+        @pl.when(i > 0)
+        def _():
+            mixed_copy(sp, 0, near(i)).wait_send()
+            mixed_copy(mirror, 1, near(i)).wait_send()
+
+        return carry
+
+    lax.fori_loop(0, half, drain_rounds, 0)
+    for k in range(1, ny):
+        yy = y_peer(k)
+        remote(tga.at[tp], tga.at[tp], ty_send.at[yy], ty_recv.at[y], (sp, tp_of(yy))).wait_send()
+    for yy in range(ny):
+        mine = tga.at[tp_of(yy)]
+        remote(mine, mine, tk_send.at[yy], tk_recv.at[yy], partner).wait_send()
+    feat_copy.wait_send()
+
+
+def publish_kernel(*refs):
+    count = len(refs) // 2
+    copies = [
+        pltpu.make_async_copy(refs[n], refs[count + n], refs[-1].at[n]) for n in range(count)
+    ]
+    for copy in copies:
+        copy.start()
+    for copy in copies:
+        copy.wait()
+
+
+def local_kernels(
+    saved_tokens, cotangent, routes, route_weights, gate_in, conv_in, value_in, conv_taps,
+    out_weight, gate_proj, up_proj, down_proj,
+):
+    tok, width = saved_tokens.shape
+    n_sp, n_tp = lax.axis_size("sp"), lax.axis_size("tp")
+    top = routes.shape[1]
+    cap = 2 * tok * top // n_sp
+    ny, half = n_tp // 2, n_sp // 2
+    quarter = width // n_tp
+    chan = gate_in.shape[1]
+    fh = gate_proj.shape[2]
+    chunk, part = width // n_sp, tok // 2
+    rows = 2 * cap
+    slots = n_sp * cap
+    dims = (n_sp, n_tp, cap, quarter, tok, width, chan, fh)
+    vmem = pl.BlockSpec(memory_space=pltpu.VMEM)
+    hbm = pl.BlockSpec(memory_space=pltpu.HBM)
+    dma = pltpu.SemaphoreType.DMA
+    struct = jax.ShapeDtypeStruct
+    def still(a):
+        return pltpu.with_memory_space_constraint(a, pltpu.HBM)
+
+    results = pl.pallas_call(
+        functools.partial(exchange_kernel, dims),
+        name="exchange",
+        out_shape=(
+            struct((1, width, fh), F32),
+            struct((1, width, fh), F32),
+            struct((1, fh, width), F32),
+            struct((chunk, chan), F32),
+            struct((tok, quarter), BF16),
+            struct((tok, chan), BF16),
+            struct((tok, chan), BF16),
+            struct((tok, chan), BF16),
+        ),
+        in_specs=[hbm] * 12,
+        out_specs=(vmem,) * 8,
+        scratch_shapes=[
+            pltpu.VMEM((n_tp, n_sp, 2, cap, quarter), BF16),
+            pltpu.VMEM((n_sp, cap, fh), BF16),
+            pltpu.VMEM((n_sp, cap, fh), BF16),
+            pltpu.VMEM((n_sp, cap, fh), BF16),
+            pltpu.VMEM((fh, slots), BF16),
+            pltpu.VMEM((2, tok), jnp.int32),
+            pltpu.VMEM((2, tok), F32),
+            pltpu.VMEM((tok, width), BF16),
+            pltpu.VMEM((tok, width), BF16),
+            pltpu.VMEM((tok, chan), BF16),
+            pltpu.VMEM((tok, chan), BF16),
+            pltpu.VMEM((tok, chan), BF16),
+            pltpu.VMEM(conv_taps.shape, F32),
+            pltpu.VMEM((width, fh), BF16),
+            pltpu.VMEM((width, fh), BF16),
+            pltpu.VMEM((fh, width), BF16),
+            pltpu.VMEM((width, chan), BF16),
+            pltpu.VMEM((n_sp, cap, tok), BF16),
+            pltpu.VMEM((n_sp, 2, cap, quarter), BF16),
+            pltpu.VMEM((half, ny, rows, quarter), BF16),
+            pltpu.VMEM((2, ny, rows, quarter), F32),
+            pltpu.VMEM((half, ny, rows, quarter), BF16),
+            pltpu.VMEM((half, 2, ny, cap, quarter), BF16),
+            pltpu.VMEM((half, 2, ny, cap, quarter), BF16),
+            pltpu.VMEM((n_sp, cap, quarter), BF16),
+            pltpu.VMEM((n_sp, cap, quarter), BF16),
+            pltpu.VMEM((n_tp, tok, quarter), BF16),
+            pltpu.VMEM((tok, chan), F32),
+            pltpu.VMEM((2, 8, chan), F32),
+            pltpu.VMEM((tok, chan), F32),
+            pltpu.VMEM((2, 8, chan), F32),
+            pltpu.VMEM((tok, chan), F32),
+            pltpu.VMEM((n_sp, tok, chan), BF16),
+            pltpu.VMEM((2, n_sp, part, chunk), BF16),
+            dma((n_sp,)), dma((n_sp,)),
+            dma((ny, n_sp)), dma((ny, n_sp)),
+            dma((ny, n_sp)), dma((ny, n_sp)),
+            dma((half,)), dma((half,)),
+            dma((half, 2, ny)), dma((half, 2, ny)),
+            dma((n_sp,)), dma((n_sp,)),
+            dma((ny,)), dma((ny,)),
+            dma((ny,)), dma((ny,)),
+            dma((2, 2)), dma((2, 2)),
+            dma((2, n_sp)), dma((n_sp,)),
+            dma((n_sp,)), dma((n_sp,)),
+            dma((1,)), dma((1,)),
+            dma((12,)),
+        ],
+        compiler_params=pltpu.CompilerParams(collective_id=0, has_side_effects=True, vmem_limit_bytes=39 << 20),
+    )(
+        *map(still, (
+            routes.T, route_weights.T, saved_tokens, cotangent, gate_in, conv_in, value_in, conv_taps,
+            out_weight, gate_proj, up_proj, down_proj,
+        )),
+    )
+    return pl.pallas_call(
+        publish_kernel,
+        name="publish",
+        out_shape=tuple(struct(a.shape, a.dtype) for a in results),
+        in_specs=[vmem] * len(results),
+        out_specs=(hbm,) * len(results),
+        scratch_shapes=[dma((len(results),))],
+        compiler_params=pltpu.CompilerParams(vmem_limit_bytes=16 << 20),
+    )(*results)
 
 
 def contract_rows(left, right):
@@ -73,7 +703,7 @@
     return whole
 
 
-def local(
+def local_collectives(
     saved_tokens,
     cotangent,
     routes,
@@ -199,6 +829,22 @@
     )
 
 
+def local(*arrays):
+    tok, width = arrays[0].shape
+    n_sp, n_tp = lax.axis_size("sp"), lax.axis_size("tp")
+    cap = 2 * tok * arrays[2].shape[1] // n_sp
+    aligned = (
+        arrays[2].shape[1] == 2
+        and n_tp % 2 == 0
+        and cap % 16 == 0
+        and n_sp % 2 == 0
+        and tok % 32 == 0
+        and width % (128 * n_sp) == 0
+        and n_sp % n_tp == 0
+    )
+    return (local_kernels if aligned else local_collectives)(*arrays)
+
+
 def solution(mesh):
     in_specs = (
         P("sp", None),

time: 217 us -> 105 us (0.48)
  Pallas kernels: 0 us -> 104 us
  waiting for transfers between devices: 70.4 us -> 0 us
  matrix products: 42.5 us -> 0 us
  starting transfers between devices: 41.2 us -> 0 us
  local copies, waits for them, and re-layouts: 21.8 us -> 0 us
  blocking collectives: 16.9 us -> 0 us
  between operations: 14.5 us -> 0.65 us
  other arithmetic: 8.44 us -> 0 us
    pallas_call x0 -> x2, Pallas kernels: none -> 104 us  [the longest x1 99.1 us: local_kernels(): pl.pallas_call(functools.partial(exchange_kernel, dims), name='exchange',...]
    dot_general x14 -> x0, matrix products: 42.5 us -> none  [the longest x5 22.6 us: contract_rows(): lax.dot_general(left, right, (((0,), (0,)), ((), ())), preferred_element_...]
    ppermute x13 -> x0, waiting for transfers between devices: 39 us -> none  [the longest x1 18.6 us: exchange_groups(): got = lax.ppermute(sums[step - 1].astype(jnp.bfloat16), 'tp', moves)]
    all_to_all x4 -> x0, waiting for transfers between devices: 30.8 us -> none  [the longest x3 29.6 us: dispatched(): return lax.all_to_all(rows, 'sp', split_axis=0, concat_axis=0, tiled=True)]
    all_to_all x4 -> x0, starting transfers between devices: 24.2 us -> none  [the longest x3 20.5 us: dispatched(): return lax.all_to_all(rows, 'sp', split_axis=0, concat_axis=0, tiled=True)]
    all_gather x2 -> x0, blocking collectives: 16.9 us -> none  [the longest x1 8.84 us: local(): features = lax.all_gather(quarter, 'tp', axis=1, tiled=True)]
    ppermute x13 -> x0, starting transfers between devices: 16.8 us -> none  [the longest x2 8.46 us: halo(): lax.ppermute(cells[-1:], axis, [(i, (i + 1) % count) for i in range(ends)])]
    dynamic_update_slice x8 -> x0, local copies, waits for them, and re-layouts: 9.13 us -> none  [the longest x4 4.62 us: gather_features(): lax.dynamic_update_slice_in_dim(whole, twins[step], (first + 1 - side) *...]
  transfers between devices with their start and end apart: 18 -> 0, of which waited for: 7 -> 0; matrix products, arithmetic and copies ran while one was open for 23% -> 0% of each run, Pallas kernels for 0% -> 0%
where the time goes in v2:
time: 105 us
  Pallas kernels  104 us (99%)
    pallas_call x1, Pallas kernels, local_kernels(): pl.pallas_call(functools.partial(exchange_kernel, dims), name='exchange',...  99.1 us
    pallas_call x1, Pallas kernels, local_kernels(): pl.pallas_call(publish_kernel, name='publish', out_shape=tuple((struct(a....  4.82 us

profile of v2, /device:TPU:0, one launch (start us, length us, event | category | flops | bytes accessed | tf_op | source)
XLA Modules:
  0.0 104.6 jit_solution(14745030691858648488)
XLA Ops:
  0.6 99.1 %exchange.1 = (f32[1,2048,512]{2,1,0:T(8,128)S(1)}, f32[1,2048,512]{2,1,0:T(8,128)S(1)}, f32[1,512,2048]{2,1,0:T(8,128)S(1)}, f32[256,256]{1,0:T(8,128)S(1)}, bf...) custom-call(s32[2,192]{1,0:T(2,128)} %bitcast.2, ...), custom_call_target="tpu_custom_call" | custom-call | tf_op jit(solution)/shard_map/exchange/pallas_call | solution.py:558
  99.8 4.8 %publish.1 = (f32[1,2048,512]{2,1,0:T(8,128)}, f32[1,2048,512]{2,1,0:T(8,128)}, f32[1,512,2048]{2,1,0:T(8,128)}, f32[256,256]{1,0:T(8,128)}, bf16[192,512]{1,0:T...) custom-call(f32[1,2048,512]{2,1,0:T(8,128)S(1)} %get-tuple-element.16.refs_0_, ...), custom_call_target="tpu_custom_call" | custom-call | tf_op jit(solution)/shard_map/publish/pallas_call | solution.py:629

commit v3 on v2

--- a/solution.py
+++ b/solution.py
@@ -131,11 +131,23 @@
         place[d] = picked
         return picked, scale
 
-    def send_block(d):
+    def block_copy(d, yy):
+        return remote(
+            sendb.at[d, yy], x_ref.at[tp_of(yy), sp], a_send.at[d, yy], a_recv.at[sp, yy], (d, tp)
+        )
+
+    def block_landing(s, yy):
+        landed = x_ref.at[tp_of(yy), s]
+        return remote(landed, landed, a_send.at[s, yy], a_recv.at[s, yy], (s, tp))
+
+    def send_block(d, features):
         picked, scale = placed(d)
-        sendb[d, 0] = rows_dot(picked, tokens_ref[:, own]).astype(BF16)
-        sendb[d, 1] = (rows_dot(picked, cot_ref[:, own]) * scale).astype(BF16)
-        remote(sendb.at[d], x_ref.at[tp, sp], a_send.at[d], a_recv.at[sp], (d, tp)).start()
+        for k in features:
+            yy = y_peer(k)
+            at = pl.ds(pl.multiple_of(tp_of(yy) * quarter, quarter), quarter)
+            sendb[d, yy, 0] = rows_dot(picked, tokens_ref[:, at]).astype(BF16)
+            sendb[d, yy, 1] = (rows_dot(picked, cot_ref[:, at]) * scale).astype(BF16)
+            block_copy(d, yy).start()
 
     for load in early:
         load.wait()
@@ -199,12 +211,11 @@
 
 
     def dispatch(r):
-        send_block(far(r))
-        pl.when(r + 1 < half)(lambda: send_block(near(r + 1)))
+        send_block(far(r), range(1))
+        pl.when(r + 1 < half)(lambda: send_block(near(r + 1), range(ny)))
 
     def dispatched(r):
-        d = far(r)
-        remote(sendb.at[d], sendb.at[d], a_send.at[d], a_recv.at[d], (d, tp)).wait_send()
+        block_copy(far(r), y).wait_send()
 
     for r in range(min(AHEAD, half)):
         dispatch(r)
@@ -215,22 +226,22 @@
         x_ref[q, sp, 0] = rows_dot(picked, tokens_ref[:, at]).astype(BF16)
         x_ref[q, sp, 1] = (rows_dot(picked, cot_ref[:, at]) * scale).astype(BF16)
 
-    halo_finish(prod, halo_p, 0)
-    above, below = shifted(prod[...], halo_p)
-    conv_out = tap0 * above + tap1 * prod[...] + tap2 * below
-    conv_s[...] = conv_out
-    mixed[sp] = (gate_f * conv_out).astype(BF16)
-
     def mixed_copy(b, which, d):
         return remote(mixed.at[b], mixed.at[b], m_send.at[which, d], m_recv.at[b], (d, tp))
 
-    mixed_copy(sp, 0, mirror).start()
-
-    def spread_own(r, carry):
-        mixed_copy(sp, 0, near(r)).start()
-        return carry
-
-    lax.fori_loop(1, half, spread_own, 0)
+    def spread_own():
+        halo_finish(prod, halo_p, 0)
+        above, below = shifted(prod[...], halo_p)
+        conv_out = tap0 * above + tap1 * prod[...] + tap2 * below
+        conv_s[...] = conv_out
+        mixed[sp] = (gate_f * conv_out).astype(BF16)
+        mixed_copy(sp, 0, mirror).start()
+
+        def one(r, carry):
+            mixed_copy(sp, 0, near(r)).start()
+            return carry
+
+        lax.fori_loop(1, half, one, 0)
 
     def spread_mirror():
         mixed_copy(mirror, 0, mirror).wait_recv()
@@ -241,30 +252,39 @@
 
         lax.fori_loop(1, half, one, 0)
 
-    def land(s):
+    def to_partner(yy, s):
+        landed = x_ref.at[tp_of(yy), s]
+        return remote(landed, landed, k_send.at[yy, s], k_recv.at[yy, s], partner)
+
+    def to_y_peer(yy, s):
         landed = x_ref.at[tp, s]
-        remote(landed, landed, a_send.at[s], a_recv.at[s], (s, tp)).wait_recv()
+        return remote(landed, landed, y_send.at[yy, s], y_recv.at[y, s], (sp, tp_of(yy)))
+
+    def land_near(s):
+        for k in range(ny):
+            block_landing(s, y_peer(k)).wait_recv()
+            to_partner(y_peer(k), s).start()
+
+    def land_far(s):
+        block_landing(s, y).wait_recv()
         for k in range(1, ny):
-            yy = y_peer(k)
-            remote(landed, landed, y_send.at[yy, s], y_recv.at[y, s], (sp, tp_of(yy))).start()
-        remote(landed, landed, k_send.at[y, s], k_recv.at[y, s], partner).start()
+            to_y_peer(y_peer(k), s).start()
+        to_partner(y, s).start()
 
     def arrive(i):
         dispatched(i)
         pl.when(i + AHEAD < half)(lambda: dispatch(i + AHEAD))
-        pl.when(i + 1 < half)(lambda: land(near(-i - 1)))
-        land(far(-i))
-
-    def pass_on(s):
+        pl.when(i == half - 1)(spread_own)
+        pl.when(i + 1 < half)(lambda: land_near(near(-i - 1)))
+        land_far(far(-i))
+
+    def relay(i):
+        s = far(-i)
         for k in range(1, ny):
             yy = y_peer(k)
             landed = x_ref.at[tp_of(yy), s]
             remote(landed, landed, y_send.at[yy, s], y_recv.at[yy, s], (sp, tp_of(yy))).wait_recv()
-            remote(landed, landed, k_send.at[yy, s], k_recv.at[yy, s], partner).start()
-
-    def relay(i):
-        pl.when(i + 1 < half)(lambda: pass_on(near(-i - 1)))
-        pass_on(far(-i))
+            to_partner(yy, s).start()
 
     def complete(s):
         for yy in range(ny):
@@ -367,7 +387,6 @@
         pl.when((i >= 2) & (i < half + 2))(lambda: compute(i - 2))
         pl.when((i >= 1) & (i < half + 1))(lambda: relay(i - 1))
         pl.when((i >= 2) & (i < half + 2))(lambda: reduce_cores(i - 2))
-        pl.when(i == half)(spread_mirror)
         pl.when(i >= 3)(lambda: give_back(i - 3))
         return carry
 
@@ -398,6 +417,7 @@
         yy = y_peer(k)
         remote(tga.at[tp], tga.at[tp], ty_send.at[yy], ty_recv.at[y], (sp, tp_of(yy))).start()
     remote(tga.at[tp], tga.at[tp], tk_send.at[y], tk_recv.at[y], partner).start()
+    spread_mirror()
     input_grads(1)
     for k in range(1, ny):
         yy = y_peer(k)
@@ -481,18 +501,22 @@
 
     def drain(n, carry):
         d = (sp + n) % n_sp
-        pl.when((d // half == side) & (d != sp))(
-            lambda: remote(sendb.at[d], sendb.at[d], a_send.at[d], a_recv.at[d], (d, tp)).wait_send()
-        )
+        beside = d // half == side
+
+        @pl.when(beside)
+        def _():
+            for yy in range(ny):
+                block_copy(d, yy).wait_send()
+
+        @pl.when(jnp.logical_not(beside))
+        def _():
+            for k in range(1, ny):
+                to_y_peer(y_peer(k), d).wait_send()
+
+        for yy in range(ny):
+            to_partner(yy, d).wait_send()
         remote(share.at[d], share.at[d], r_send.at[d], r_recv.at[d], (d, tp)).wait_send()
         remote(feature_of(d), feat.at[c, sp], o_send.at[d], o_recv.at[d], (d, tp)).wait_send()
-        for k in range(1, ny):
-            yy = y_peer(k)
-            mine = x_ref.at[tp, d]
-            remote(mine, mine, y_send.at[yy, d], y_recv.at[yy, d], (sp, tp_of(yy))).wait_send()
-        for yy in range(ny):
-            mine = x_ref.at[tp_of(yy), d]
-            remote(mine, mine, k_send.at[yy, d], k_recv.at[yy, d], partner).wait_send()
         return carry
 
     lax.fori_loop(1, n_sp, drain, 0)
@@ -589,7 +613,7 @@
             pltpu.VMEM((fh, width), BF16),
             pltpu.VMEM((width, chan), BF16),
             pltpu.VMEM((n_sp, cap, tok), BF16),
-            pltpu.VMEM((n_sp, 2, cap, quarter), BF16),
+            pltpu.VMEM((n_sp, ny, 2, cap, quarter), BF16),
             pltpu.VMEM((half, ny, rows, quarter), BF16),
             pltpu.VMEM((2, ny, rows, quarter), F32),
             pltpu.VMEM((half, ny, rows, quarter), BF16),
@@ -605,7 +629,7 @@
             pltpu.VMEM((tok, chan), F32),
             pltpu.VMEM((n_sp, tok, chan), BF16),
             pltpu.VMEM((2, n_sp, part, chunk), BF16),
-            dma((n_sp,)), dma((n_sp,)),
+            dma((n_sp, ny)), dma((n_sp, ny)),
             dma((ny, n_sp)), dma((ny, n_sp)),
             dma((ny, n_sp)), dma((ny, n_sp)),
             dma((half,)), dma((half,)),
@@ -619,7 +643,7 @@
             dma((1,)), dma((1,)),
             dma((12,)),
         ],
-        compiler_params=pltpu.CompilerParams(collective_id=0, has_side_effects=True, vmem_limit_bytes=39 << 20),
+        compiler_params=pltpu.CompilerParams(collective_id=0, has_side_effects=True, vmem_limit_bytes=41 << 20),
     )(
         *map(still, (
             routes.T, route_weights.T, saved_tokens, cotangent, gate_in, conv_in, value_in, conv_taps,

time: 105 us -> 102 us (0.971)
  Pallas kernels: 104 us -> 101 us
    pallas_call x1, Pallas kernels: 99.1 us -> 96.2 us  [local_kernels(): pl.pallas_call(functools.partial(exchange_kernel, dims), name='exchange',...]
where the time goes in v3:
time: 102 us
  Pallas kernels  101 us (99%)
    pallas_call x1, Pallas kernels, local_kernels(): pl.pallas_call(functools.partial(exchange_kernel, dims), name='exchange',...  96.2 us
    pallas_call x1, Pallas kernels, local_kernels(): pl.pallas_call(publish_kernel, name='publish', out_shape=tuple((struct(a....  4.82 us

profile of v3, /device:TPU:0, one launch (start us, length us, event | category | flops | bytes accessed | tf_op | source)
XLA Modules:
  0.0 101.6 jit_solution(10951168875430651601)
XLA Ops:
  0.6 96.2 %exchange.1 = (f32[1,2048,512]{2,1,0:T(8,128)S(1)}, f32[1,2048,512]{2,1,0:T(8,128)S(1)}, f32[1,512,2048]{2,1,0:T(8,128)S(1)}, f32[256,256]{1,0:T(8,128)S(1)}, bf...) custom-call(s32[2,192]{1,0:T(2,128)} %bitcast.2, ...), custom_call_target="tpu_custom_call" | custom-call | tf_op jit(solution)/shard_map/exchange/pallas_call | solution.py:582
  96.8 4.8 %publish.1 = (f32[1,2048,512]{2,1,0:T(8,128)}, f32[1,2048,512]{2,1,0:T(8,128)}, f32[1,512,2048]{2,1,0:T(8,128)}, f32[256,256]{1,0:T(8,128)}, bf16[192,512]{1,0:T...) custom-call(f32[1,2048,512]{2,1,0:T(8,128)S(1)} %get-tuple-element.16.refs_0_, ...), custom_call_target="tpu_custom_call" | custom-call | tf_op jit(solution)/shard_map/publish/pallas_call | solution.py:653
